TPU v7x, 128 devices: a 2x2x16 block of a 8x8x16 slice. The times are simulated.
128 devices in a mesh: grp: 4 (over y, x), ep: 32 (over z, core).
Axes of the slice: x: 2, y: 2, z: 16, core: 2. Of those that a mesh axis runs over, the one named last changes fastest.
The devices are a block of a 8x8x16 slice.
Arguments:
- hidden: bfloat16 [384, 2048], P(('grp', 'ep')), parts along dimension 0, may hold values from -6 to 6
- conv_window: bfloat16 [384, 3, 6144], P(('grp', 'ep')), parts along dimension 0, may hold values from -6 to 6
- ssm_state: float32 [384, 64, 64, 128], P(('grp', 'ep')), parts along dimension 0, may hold values from -1.75 to 1.75
- gate_proj: bfloat16 [2048, 4096], P(None, 'ep'), may hold values from -0.125 to 0.125
- input_proj: bfloat16 [2048, 4096], P(None, 'ep'), may hold values from -0.125 to 0.125
- write_proj: bfloat16 [2048, 1024], P(None, 'ep'), may hold values from -0.125 to 0.125
- read_proj: bfloat16 [2048, 1024], P(None, 'ep'), may hold values from -0.125 to 0.125
- step_proj: bfloat16 [2048, 64], replicated, may hold values from -0.125 to 0.125
- step_bias: float32 [64], replicated, may hold values from -2 to 1
- decay_log: float32 [64], replicated, may hold values from -2.3 to 1.4
- decay_shift: float32 [384, 64], P(('grp', 'ep')), parts along dimension 0, may hold values from -0.7 to 0
- skip_scale: float32 [64], replicated, may hold values from -4 to 4
- conv_taps: bfloat16 [4, 6144], replicated, may hold values from -3 to 3
- conv_bias: float32 [6144], replicated, may hold values from -3 to 3
- mix_gain: float32 [2048], replicated, may hold values from 0.1 to 1.9
- group_gain: float32 [4096], replicated, may hold values from 0.1 to 1.9
- out_proj: bfloat16 [4096, 2048], P(None, 'ep'), may hold values from -0.09375 to 0.09375
- ffn_gain: float32 [2048], replicated, may hold values from 0.1 to 1.9
- router: bfloat16 [2048, 32], replicated, may hold values from -0.125 to 0.125
- expert_ids: int32 [384, 6], P(('grp', 'ep')), parts along dimension 0, may hold values from 0 to 31, all different within a row; in each aligned block of 3 rows (0 to 2, 3 to 5, ...) at most 2 rows name the same one
- expert_gate: bfloat16 [32, 2048, 512], P('ep'), may hold values from -0.125 to 0.125
- expert_up: bfloat16 [32, 2048, 512], P('ep'), may hold values from -0.125 to 0.125
- expert_down: bfloat16 [32, 512, 2048], P('ep'), may hold values from -0.25 to 0.25
- shared_gate: bfloat16 [2048, 512], P('ep'), may hold values from -0.125 to 0.125
- shared_up: bfloat16 [2048, 512], P('ep'), may hold values from -0.125 to 0.125
- shared_down: bfloat16 [512, 2048], replicated, may hold values from -0.25 to 0.25
Outputs:
- layer_out: bfloat16 [384, 2048], P(('grp', 'ep')), parts along dimension 0
- next_state: float32 [384, 64, 64, 128], P(('grp', 'ep')), parts along dimension 0
- next_window: bfloat16 [384, 3, 6144], P(('grp', 'ep')), parts along dimension 0
There are 4 independent parts, one for each index of `grp`. A program takes and returns all parts, laid end to end along the dimension named above; an argument that names none is the same for every part. Nothing has to cross between parts.
Inputs may be any that keep to these rules, and one draw needn't show every extreme that they name: `expert_ids`: each row names 6 different experts; in the rows of one device no expert is named by more than 2 rows, and in every draw some device's rows name some expert exactly 2 times.
All inputs are finite; a program needn't handle non-finite values.
Results may differ from a plain program's by a relative error of at most 0.019.
Values may be sent and summed in bfloat16 or wider, within the bound.
A program may use at most 128 MiB of HBM per device.

v0:
```python
import jax
import jax.numpy as jnp
from jax import lax
from jax.sharding import Mesh
from jax.sharding import PartitionSpec as P

HEAD_DIM = 64
GROUPS = 8
STATE = 128
CAP = 2
EP = ("ep_0", "ep_1")
GRP_EP = ("grp", "ep_0", "ep_1")


epsilon = 1e-06
routed_scale = 2.5


def from_everyone(shard, axis):
    count = lax.axis_size(axis)
    return lax.all_to_all(
        jnp.broadcast_to(shard[None], (count, *shard.shape)), axis, 0, 0, tiled=True
    )


def in_order(pieces, dim):
    dims = list(pieces.shape[1:])
    dims[dim] *= pieces.shape[0]
    return jnp.moveaxis(pieces, 0, dim).reshape(dims)


def gathered_copies(shard, axis, dim):
    pieces = from_everyone(shard, axis)
    return in_order(pieces, dim)


def all_blocks(shard, axes, turns):
    pieces = shard
    for k in turns:
        pieces = lax.all_gather(pieces, axes[k])
    done = turns[::-1]
    back = [done.index(k) for k in range(len(axes))]
    pieces = pieces.transpose(*back, *range(len(axes), pieces.ndim))
    return pieces.reshape(-1, *shard.shape)


def whole_of(shard, axes, turns, dim):
    return in_order(all_blocks(shard, axes, turns), dim)


def cut_along(shard, dim, count):
    before, after = (shard.shape[:dim], shard.shape[dim + 1 :])
    return jnp.moveaxis(shard.reshape(*before, count, -1, *after), dim, 0)


def summed_on_arrival(shard, axis, dim):
    pieces = cut_along(shard, dim, lax.axis_size(axis))
    arrived = lax.all_to_all(pieces, axis, split_axis=0, concat_axis=0, tiled=True)
    return arrived.astype(jnp.float32).sum(axis=0)


def row_scale(values):
    return lax.rsqrt(jnp.mean(values * values, axis=-1, keepdims=True) + epsilon)


def matmul(left, right):
    return jnp.dot(left, right, preferred_element_type=jnp.float32)


def expert_result(rows_in, weight_gate, weight_up, weight_down):
    expert_hidden = (jax.nn.silu(matmul(rows_in, weight_gate)) * matmul(rows_in, weight_up)).astype(
        jnp.bfloat16
    )
    return matmul(expert_hidden, weight_down).astype(jnp.bfloat16)


def route_weights(routed_in, router, chosen):
    scores = jax.nn.sigmoid(matmul(routed_in, router))
    picked = jnp.take_along_axis(scores, chosen, axis=1)
    return routed_scale * picked / jnp.sum(picked, axis=1, keepdims=True)


def shards(
    hidden,
    conv_window,
    ssm_state,
    gate_proj,
    input_proj,
    write_proj,
    read_proj,
    step_proj,
    step_bias,
    decay_log,
    decay_shift,
    skip_scale,
    conv_taps,
    conv_bias,
    mix_gain,
    group_gain,
    out_proj,
    ffn_gain,
    router,
    expert_ids,
    expert_gate,
    expert_up,
    expert_down,
    shared_gate,
    shared_up,
    shared_down,
):
    local_rows = hidden.shape[0]
    device_index = lax.axis_index(EP)
    gathered = gathered_copies(hidden, EP, 0)
    gathered_wide = gathered.astype(jnp.float32)
    normed = (gathered_wide * row_scale(gathered_wide) * mix_gain).astype(jnp.bfloat16)
    gate_part = matmul(normed, gate_proj).astype(jnp.bfloat16)
    input_part = matmul(normed, input_proj).astype(jnp.bfloat16)
    write_part = matmul(normed, write_proj).astype(jnp.bfloat16)
    read_part = matmul(normed, read_proj).astype(jnp.bfloat16)
    gate_rows, input_rows, write_rows, read_rows = (
        lax.all_to_all(gate_part, EP, split_axis=0, concat_axis=1, tiled=True),
        lax.all_to_all(input_part, EP, split_axis=0, concat_axis=1, tiled=True),
        lax.all_to_all(write_part, EP, split_axis=0, concat_axis=1, tiled=True),
        lax.all_to_all(read_part, EP, split_axis=0, concat_axis=1, tiled=True),
    )
    normed_local = lax.dynamic_slice_in_dim(normed, device_index * local_rows, local_rows, 0)
    step_raw = matmul(normed_local, step_proj)
    inner_width = gate_rows.shape[1]
    state_span = GROUPS * STATE
    head_count = step_bias.shape[0]
    per_group = head_count // GROUPS
    fresh_row = jnp.concatenate([input_rows, write_rows, read_rows], axis=1)
    window = jnp.concatenate([conv_window, fresh_row[:, None, :]], axis=1)
    convolved = jax.nn.silu(
        jnp.sum(window.astype(jnp.float32) * conv_taps.astype(jnp.float32)[None], axis=1)
        + conv_bias
    )
    head_input = convolved[:, :inner_width].reshape(local_rows, GROUPS, per_group, HEAD_DIM)
    write_vec = convolved[:, inner_width : inner_width + state_span].reshape(
        local_rows, GROUPS, STATE
    )
    read_vec = convolved[:, inner_width + state_span :].reshape(local_rows, GROUPS, STATE)
    step_size = jax.nn.softplus(step_raw + step_bias)
    decay_rate = jnp.exp(decay_shift - step_size * jnp.exp(decay_log)).reshape(
        local_rows, GROUPS, per_group
    )
    step_group = step_size.reshape(local_rows, GROUPS, per_group)
    carried = ssm_state.reshape(local_rows, GROUPS, per_group, HEAD_DIM, STATE)
    next_state = (
        decay_rate[..., None, None] * carried
        + (step_group[..., None] * head_input)[..., None] * write_vec[:, :, None, None, :]
    )
    mixed_out = jnp.einsum("sgepn,sgn->sgep", next_state, read_vec)
    mixed_out = mixed_out + skip_scale.reshape(GROUPS, per_group)[None, :, :, None] * head_input
    mixed_out = mixed_out.reshape(local_rows, inner_width).astype(jnp.bfloat16)
    gated_out = mixed_out.astype(jnp.float32) * jax.nn.silu(gate_rows.astype(jnp.float32))
    blocks = gated_out.reshape(local_rows, GROUPS, -1)
    gated_out = ((blocks * row_scale(blocks)).reshape(local_rows, inner_width) * group_gain).astype(
        jnp.bfloat16
    )
    col_width = out_proj.shape[1]
    resid_cols = lax.dynamic_slice_in_dim(gathered_wide, device_index * col_width, col_width, 1)
    resid_part = (resid_cols + matmul(whole_of(gated_out, EP, (0, 1), 0), out_proj)).astype(
        jnp.bfloat16
    )
    gain_part = lax.dynamic_slice_in_dim(ffn_gain, device_index * col_width, col_width, 0)
    shared_part = (resid_part.astype(jnp.float32) * gain_part).astype(jnp.bfloat16)
    shared_pre = summed_on_arrival(
        jnp.concatenate(
            [matmul(shared_part, shared_gate), matmul(shared_part, shared_up)], axis=1
        ).astype(jnp.bfloat16),
        EP,
        0,
    )
    exp_dev = expert_gate.shape[0]
    resid = lax.all_to_all(resid_part, EP, split_axis=0, concat_axis=1, tiled=True)
    resid_wide = resid.astype(jnp.float32)
    norm_scale = row_scale(resid_wide)
    routed_in = (resid_wide * norm_scale * ffn_gain).astype(jnp.bfloat16)
    weights = route_weights(routed_in, router, expert_ids)
    expert_total = router.shape[1]
    member = jnp.any(
        expert_ids[:, :, None] == jnp.arange(expert_total, dtype=jnp.int32)[None, None, :], axis=1
    ).astype(jnp.int32)
    earlier = jnp.cumsum(member, axis=0) - member
    slot_index = jnp.take_along_axis(earlier, expert_ids, axis=1)
    places = expert_ids * CAP + slot_index
    dispatch_table = jnp.any(
        places[None, :, :] == jnp.arange(expert_total * CAP, dtype=jnp.int32)[:, None, None], axis=2
    ).astype(jnp.bfloat16)
    outbound = (
        matmul(dispatch_table, routed_in)
        .astype(jnp.bfloat16)
        .reshape(lax.axis_size(EP), exp_dev, CAP, routed_in.shape[1])
    )
    arrived = lax.all_to_all(outbound, EP, split_axis=0, concat_axis=0, tiled=True)
    rows_in = arrived[:, 0].reshape(-1, arrived.shape[-1])
    result = expert_result(rows_in, expert_gate[0], expert_up[0], expert_down[0])
    results = [result.reshape(arrived.shape[0], arrived.shape[2], arrived.shape[3])]
    returned = lax.all_to_all(
        jnp.stack(results, axis=1), EP, split_axis=0, concat_axis=0, tiled=True
    )
    returned_flat = returned.reshape(expert_total * CAP, returned.shape[-1])
    picked = jnp.take(returned_flat, places.reshape(-1), axis=0).reshape(
        local_rows, expert_ids.shape[1], returned.shape[-1]
    )
    routed = jnp.sum(picked.astype(jnp.float32) * weights[:, :, None], axis=1)
    hidden_units = shared_down.shape[0]
    shared_hidden = (
        jax.nn.silu(norm_scale * shared_pre[:, :hidden_units])
        * (norm_scale * shared_pre[:, hidden_units:])
    ).astype(jnp.bfloat16)
    layer_out = (resid_wide + routed + matmul(shared_hidden, shared_down)).astype(jnp.bfloat16)
    return (layer_out, next_state.reshape(ssm_state.shape), window[:, 1:])


def solution(mesh):
    torus = Mesh(mesh.devices.reshape(mesh.shape["grp"], 16, 2), ("grp", "ep_0", "ep_1"))
    return jax.shard_map(
        shards,
        mesh=torus,
        in_specs=(
            P(GRP_EP, None),
            P(GRP_EP, None, None),
            P(GRP_EP, None, None, None),
            P(None, EP),
            P(None, EP),
            P(None, EP),
            P(None, EP),
            P(),
            P(),
            P(),
            P(GRP_EP, None),
            P(),
            P(),
            P(),
            P(),
            P(),
            P(None, EP),
            P(),
            P(),
            P(GRP_EP, None),
            P(EP, None, None),
            P(EP, None, None),
            P(EP, None, None),
            P(EP, None),
            P(EP, None),
            P(),
        ),
        out_specs=(P(GRP_EP, None), P(GRP_EP, None, None, None), P(GRP_EP, None, None)),
        check_vma=False,
    )
```

profile of v0, /device:TPU:86, one launch (start us, length us, event | category | flops | bytes accessed | tf_op | source)
XLA Modules:
  0.0 272.0 jit_solution(13049437831377829950)
XLA Ops:
  0.7 1.9 broadcast_in_dim.11
  2.6 17.8 %all-to-all-start = ((bf16[32,3,2048]{2,1,0:T(4,128)(2,1)}), bf16[32,3,2048]{2,1,0:T(4,128)(2,1)S(1)}, u32[]{:S(2)}, u32[]{:S(2)}) async-start(bf16[32,3,2048]{2,1,0:T(4,128)(2,1)} %broadcast_in_dim.11), calls=%async_computation | async-start | bytes 1048576 | tf_op jit(solution)/shard_map/all_to_all | solution.py:21
  20.4 0.8 convert_element_type.157
  21.2 0.7 exp.42
  21.9 1.3 mul.284
  23.2 0.8 fusion.41
  24.0 0.7 bitcast_or_fusion
  24.8 0.8 gather_fusion.1
  25.7 1.2 compare_and_fusion
  27.0 1.3 dynamic_slice.11
  28.4 0.6 pad_clamp_fusion
  28.9 0.6 fusion.42
  29.6 23.9 %all-to-all-done = bf16[32,3,2048]{2,1,0:T(4,128)(2,1)S(1)} async-done(((bf16[32,3,2048]{2,1,0:T(4,128)(2,1)}), bf16[32,3,2048]{2,1,0:T(4,128)(2,1)S(1)}, u32[]{:S(2)}, u32[]{:S(2)}) %all-to-all-start) | async-done | bytes 393248 | tf_op jit(solution)/shard_map/all_to_all | solution.py:21
  53.5 0.4 multiply_reduce_fusion
  53.9 0.3 reshape.278
  54.2 0.8 multiply_convert_fusion
  55.1 1.1 convolution_convert_fusion.7
  56.4 0.7 all_to_all.79
  57.0 4.8 %all-to-all-start.2 = ((bf16[32,3,32]{2,1,0:T(4,128)(2,1)}), bf16[32,3,32]{2,1,0:T(4,128)(2,1)S(1)}, u32[]{:S(2)}, u32[]{:S(2)}) async-start(bf16[32,3,32]{2,1,0:T(4,128)(2,1)} %all_to_all.79), calls=%async_computation.2 | async-start | bytes 65536 | tf_op jit(solution)/shard_map/all_to_all | solution.py:123
  61.8 1.3 convolution_convert_fusion.5
  63.1 1.3 convolution_convert_fusion.4
  64.4 1.1 convolution_convert_fusion.6
  65.7 0.7 all_to_all.83
  66.3 7.6 %all-to-all-done.2 = bf16[32,3,32]{2,1,0:T(4,128)(2,1)S(1)} async-done(((bf16[32,3,32]{2,1,0:T(4,128)(2,1)}), bf16[32,3,32]{2,1,0:T(4,128)(2,1)S(1)}, u32[]{:S(2)}, u32[]{:S(2)}) %all-to-all-start.2) | async-done | bytes 6176 | tf_op jit(solution)/shard_map/all_to_all | solution.py:123
  73.9 4.8 %all-to-all-start.3 = ((bf16[32,3,32]{2,1,0:T(4,128)(2,1)}), bf16[32,3,32]{2,1,0:T(4,128)(2,1)S(1)}, u32[]{:S(2)}, u32[]{:S(2)}) async-start(bf16[32,3,32]{2,1,0:T(4,128)(2,1)} %all_to_all.83), calls=%async_computation.3 | async-start | bytes 65536 | tf_op jit(solution)/shard_map/all_to_all | solution.py:124
  78.7 1.1 subtract_exponential_fusion
  79.9 0.6 all_to_all.75
  80.7 0.6 all_to_all.87
  81.3 9.7 %all-to-all-done.3 = bf16[32,3,32]{2,1,0:T(4,128)(2,1)S(1)} async-done(((bf16[32,3,32]{2,1,0:T(4,128)(2,1)}), bf16[32,3,32]{2,1,0:T(4,128)(2,1)S(1)}, u32[]{:S(2)}, u32[]{:S(2)}) %all-to-all-start.3) | async-done | bytes 6176 | tf_op jit(solution)/shard_map/all_to_all | solution.py:124
  91.0 4.7 %all-to-all-start.1 = ((bf16[32,3,128]{2,1,0:T(4,128)(2,1)}), bf16[32,3,128]{2,1,0:T(4,128)(2,1)S(1)}, u32[]{:S(2)}, u32[]{:S(2)}) async-start(bf16[32,3,128]{2,1,0:T(4,128)(2,1)} %all_to_all.75), calls=%async_computation.1 | async-start | bytes 65536 | tf_op jit(solution)/shard_map/all_to_all | solution.py:122
  96.1 11.8 %all-to-all-done.1 = bf16[32,3,128]{2,1,0:T(4,128)(2,1)S(1)} async-done(((bf16[32,3,128]{2,1,0:T(4,128)(2,1)}), bf16[32,3,128]{2,1,0:T(4,128)(2,1)S(1)}, u32[]{:S(2)}, u32[]{:S(2)}) %all-to-all-start.1) | async-done | bytes 24608 | tf_op jit(solution)/shard_map/all_to_all | solution.py:122
  107.9 4.8 %all-to-all-start.4 = ((bf16[32,3,128]{2,1,0:T(4,128)(2,1)}), bf16[32,3,128]{2,1,0:T(4,128)(2,1)S(1)}, u32[]{:S(2)}, u32[]{:S(2)}) async-start(bf16[32,3,128]{2,1,0:T(4,128)(2,1)} %all_to_all.87), calls=%async_computation.4 | async-start | bytes 65536 | tf_op jit(solution)/shard_map/all_to_all | solution.py:121
  112.8 1.3 multiply_reduce_fusion.1
  114.0 0.8 divide_multiply_fusion
  115.0 9.8 %all-to-all-done.4 = bf16[32,3,128]{2,1,0:T(4,128)(2,1)S(1)} async-done(((bf16[32,3,128]{2,1,0:T(4,128)(2,1)}), bf16[32,3,128]{2,1,0:T(4,128)(2,1)S(1)}, u32[]{:S(2)}, u32[]{:S(2)}) %all-to-all-start.4) | async-done | bytes 24608 | tf_op jit(solution)/shard_map/all_to_all | solution.py:121
  125.0 4.7 %fusion = f32[3,8,1,8,64]{4,2,3,1,0:T(1,128)S(1)} fusion(f32[3,8,128,1,1]{2,3,4,1,0:T(1,128)S(1)} %bitcast.105, f32[3,8,8,64,128]{4,3,2,1,0:T(8,128)} %bitcast.96, f32[3,8,128]{2,1,0:T(8,128)S(1)} %bitcast.103, f32[3,8,8,64]{3,2,1,0:T(8,128)S(1)} %broadcast_multiply_fusion.1, f32[3,8,8]{2,1,0:T(8,128)S(1)} %mul.271), kind=kOutput, calls=%fused_computation.4 | convolution fusion | flops 7864320 | bytes 6415104 | tf_op jit(solution)/shard_map/sgepn,sgn->sgep/dot_general | solution.py:153
  130.2 0.8 multiply_convert_fusion.1
  131.0 29.4 %all_gather.10 = bf16[16,3,4096]{2,1,0:T(4,128)(2,1)S(1)} all-gather(bf16[1,3,4096]{2,1,0:T(4,128)(2,1)S(1)} %multiply_convert_fusion.1), channel_id=1, replica_groups=mesh['grp'=4,'ep_0'=16,'ep_1'=2] {'ep_0'}, dimensions={0}, use_global_device_ids=true | all-gather | bytes 417792 | tf_op jit(solution)/shard_map/all_gather | solution.py:40
  160.7 2.4 all-gather
  163.1 0.7 copy.85
  163.8 1.4 reshape_reshape.3
  165.3 1.7 fusion.21
  167.0 0.7 all_to_all.89
  167.7 5.9 %all-to-all-start.5 = ((bf16[32,3,64]{2,1,0:T(4,128)(2,1)}), bf16[32,3,64]{2,1,0:T(4,128)(2,1)S(1)}, u32[]{:S(2)}, u32[]{:S(2)}) async-start(bf16[32,3,64]{2,1,0:T(4,128)(2,1)} %all_to_all.89), calls=%async_computation.5 | async-start | bytes 65536 | tf_op jit(solution)/shard_map/all_to_all | solution.py:176
  173.6 1.1 convolution_convert_fusion.3
  174.8 1.1 convolution_convert_fusion.2
  176.1 9.8 %all-to-all-done.5 = bf16[32,3,64]{2,1,0:T(4,128)(2,1)S(1)} async-done(((bf16[32,3,64]{2,1,0:T(4,128)(2,1)}), bf16[32,3,64]{2,1,0:T(4,128)(2,1)S(1)}, u32[]{:S(2)}, u32[]{:S(2)}) %all-to-all-start.5) | async-done | bytes 12320 | tf_op jit(solution)/shard_map/all_to_all | solution.py:176
  186.2 1.0 convolution_convert_fusion.1
  187.2 0.9 reshape.274
  188.1 4.8 %all-to-all-start.6 = ((bf16[32,1,2,2048]{3,2,1,0:T(2,128)(2,1)}), bf16[32,1,2,2048]{3,2,1,0:T(2,128)(2,1)S(1)}, u32[]{:S(2)}, u32[]{:S(2)}) async-start(bf16[32,1,2,2048]{3,2,1,0:T(2,128)(2,1)} %bitcast.16), calls=%async_computation.6 | async-start | bytes 524288 | tf_op jit(solution)/shard_map/all_to_all | solution.py:196
  192.9 0.8 pad_maximum_fusion
  193.8 0.9 fusion.25
  194.7 20.2 %all-to-all-done.6 = bf16[32,1,2,2048]{3,2,1,0:T(2,128)(2,1)S(1)} async-done(((bf16[32,1,2,2048]{3,2,1,0:T(2,128)(2,1)}), bf16[32,1,2,2048]{3,2,1,0:T(2,128)(2,1)S(1)}, u32[]{:S(2)}, u32[]{:S(2)}) %all-to-all-start.6) | async-done | bytes 262176 | tf_op jit(solution)/shard_map/all_to_all | solution.py:196
  214.8 4.8 %all-to-all-start.8 = ((bf16[32,3,1024]{2,1,0:T(4,128)(2,1)}), bf16[32,3,1024]{2,1,0:T(4,128)(2,1)S(1)}, u32[]{:S(2)}, u32[]{:S(2)}) async-start(bf16[32,3,1024]{2,1,0:T(4,128)(2,1)} %pad_maximum_fusion), calls=%async_computation.8 | async-start | bytes 524288 | tf_op jit(solution)/shard_map/all_to_all | solution.py:58
  219.8 2.1 fusion.11
  221.8 2.5 convolution_convert_fusion
  224.3 0.9 stack_reshape.3
  225.2 16.4 %all-to-all-done.8 = bf16[32,3,1024]{2,1,0:T(4,128)(2,1)S(1)} async-done(((bf16[32,3,1024]{2,1,0:T(4,128)(2,1)}), bf16[32,3,1024]{2,1,0:T(4,128)(2,1)S(1)}, u32[]{:S(2)}, u32[]{:S(2)}) %all-to-all-start.8) | async-done | bytes 196640 | tf_op jit(solution)/shard_map/all_to_all | solution.py:58
  241.6 4.8 %all-to-all-start.7 = ((bf16[32,1,2,2048]{3,2,1,0:T(2,128)(2,1)}), bf16[32,1,2,2048]{3,2,1,0:T(2,128)(2,1)S(1)}, u32[]{:S(2)}, u32[]{:S(2)}) async-start(bf16[32,1,2,2048]{3,2,1,0:T(2,128)(2,1)} %bitcast.20), calls=%async_computation.7 | async-start | bytes 524288 | tf_op jit(solution)/shard_map/all_to_all | solution.py:200
  246.4 7.0 %multiply_add_fusion = f32[3,64,64,128]{3,2,1,0:T(8,128)} fusion(f32[3,64,64,128]{3,2,1,0:T(8,128)} %param.28, f32[3,64,128]{2,1,0:T(8,128)S(1)} %broadcast_bitcast_fusion, f32[3,64,64]{2,1,0:T(8,128)S(1)} %broadcast_multiply_fusion, f32[3,64]{1,0:T(4,128)S(1)} %copy-done.6), kind=kLoop, calls=%fused_computation.3 | loop fusion | flops 4718592 | bytes 12731136 | tf_op jit(solution)/shard_map/add | solution.py:150
  253.6 0.9 gather_fusion.2
  254.9 13.4 %all-to-all-done.7 = bf16[32,1,2,2048]{3,2,1,0:T(2,128)(2,1)S(1)} async-done(((bf16[32,1,2,2048]{3,2,1,0:T(2,128)(2,1)}), bf16[32,1,2,2048]{3,2,1,0:T(2,128)(2,1)S(1)}, u32[]{:S(2)}, u32[]{:S(2)}) %all-to-all-start.7) | async-done | bytes 262176 | tf_op jit(solution)/shard_map/all_to_all | solution.py:200
  268.4 0.7 gather_fusion
  269.4 2.6 fusion.7
  (82 shorter events, 4.2 us)
Async XLA Ops:
  0.6 221.2 %copy-start = (bf16[1,512,2048]{2,1,0:T(8,128)(2,1)S(1)}, bf16[1,512,2048]{2,1,0:T(8,128)(2,1)}, u32[]{:S(2)}) copy-start(bf16[1,512,2048]{2,1,0:T(8,128)(2,1)} %param.48) | copy-start | bytes 6291460
  0.6 78.1 %copy-start.11 = (f32[64]{0:T(128)S(1)}, f32[64]{0:T(128)}, u32[]{:S(2)}) copy-start(f32[64]{0:T(128)} %param.34) | copy-start | bytes 772
  0.7 78.1 %copy-start.9 = (f32[3,64]{1,0:T(4,128)S(1)}, f32[3,64]{1,0:T(4,128)}, u32[]{:S(2)}) copy-start(f32[3,64]{1,0:T(4,128)} %param.36) | copy-start | bytes 2308
  2.6 50.9 %all-to-all-start = ((bf16[32,3,2048]{2,1,0:T(4,128)(2,1)}), bf16[32,3,2048]{2,1,0:T(4,128)(2,1)S(1)}, u32[]{:S(2)}, u32[]{:S(2)}) async-start(bf16[32,3,2048]{2,1,0:T(4,128)(2,1)} %broadcast_in_dim.11), calls=%async_computation | async-start | bytes 1048576 | tf_op jit(solution)/shard_map/all_to_all | solution.py:21
  55.1 74.7 %copy-start.7 = (f32[8,8]{1,0:T(8,128)S(1)}, f32[8,8]{1,0:T(8,128)}, u32[]{:S(2)}) copy-start(f32[8,8]{1,0:T(8,128)} %mul.284) | copy-start | bytes 772
  57.0 16.9 %all-to-all-start.2 = ((bf16[32,3,32]{2,1,0:T(4,128)(2,1)}), bf16[32,3,32]{2,1,0:T(4,128)(2,1)S(1)}, u32[]{:S(2)}, u32[]{:S(2)}) async-start(bf16[32,3,32]{2,1,0:T(4,128)(2,1)} %all_to_all.79), calls=%async_computation.2 | async-start | bytes 65536 | tf_op jit(solution)/shard_map/all_to_all | solution.py:123
  73.9 17.1 %all-to-all-start.3 = ((bf16[32,3,32]{2,1,0:T(4,128)(2,1)}), bf16[32,3,32]{2,1,0:T(4,128)(2,1)S(1)}, u32[]{:S(2)}, u32[]{:S(2)}) async-start(bf16[32,3,32]{2,1,0:T(4,128)(2,1)} %all_to_all.83), calls=%async_computation.3 | async-start | bytes 65536 | tf_op jit(solution)/shard_map/all_to_all | solution.py:124
  79.9 83.2 %copy-start.3 = (f32[3,64]{1,0:T(4,128)}, f32[3,64]{1,0:T(4,128)S(1)}, u32[]{:S(2)}) copy-start(f32[3,64]{1,0:T(4,128)S(1)} %get-tuple-element.10) | copy-start | bytes 2308
  79.9 83.2 %copy-start.5 = (f32[3,64]{1,0:T(4,128)}, f32[3,64]{1,0:T(4,128)S(1)}, u32[]{:S(2)}) copy-start(f32[3,64]{1,0:T(4,128)S(1)} %get-tuple-element.9) | copy-start | bytes 2308
  91.0 16.9 %all-to-all-start.1 = ((bf16[32,3,128]{2,1,0:T(4,128)(2,1)}), bf16[32,3,128]{2,1,0:T(4,128)(2,1)S(1)}, u32[]{:S(2)}, u32[]{:S(2)}) async-start(bf16[32,3,128]{2,1,0:T(4,128)(2,1)} %all_to_all.75), calls=%async_computation.1 | async-start | bytes 65536 | tf_op jit(solution)/shard_map/all_to_all | solution.py:122
  107.9 16.9 %all-to-all-start.4 = ((bf16[32,3,128]{2,1,0:T(4,128)(2,1)}), bf16[32,3,128]{2,1,0:T(4,128)(2,1)S(1)}, u32[]{:S(2)}, u32[]{:S(2)}) async-start(bf16[32,3,128]{2,1,0:T(4,128)(2,1)} %all_to_all.87), calls=%async_computation.4 | async-start | bytes 65536 | tf_op jit(solution)/shard_map/all_to_all | solution.py:121
  129.7 64.1 %copy-start.1 = (bf16[3,3,6144]{2,1,0:T(4,128)(2,1)S(1)}, bf16[3,3,6144]{2,1,0:T(4,128)(2,1)}, u32[]{:S(2)}) copy-start(bf16[3,3,6144]{2,1,0:T(4,128)(2,1)} %param.27) | copy-start | bytes 331780
  163.1 30.6 %copy-start.4 = (f32[3,64]{1,0:T(4,128)S(1)}, f32[3,64]{1,0:T(4,128)}, u32[]{:S(2)}) copy-start(f32[3,64]{1,0:T(4,128)} %copy-done.3) | copy-start | bytes 2308
  167.7 18.2 %all-to-all-start.5 = ((bf16[32,3,64]{2,1,0:T(4,128)(2,1)}), bf16[32,3,64]{2,1,0:T(4,128)(2,1)S(1)}, u32[]{:S(2)}, u32[]{:S(2)}) async-start(bf16[32,3,64]{2,1,0:T(4,128)(2,1)} %all_to_all.89), calls=%async_computation.5 | async-start | bytes 65536 | tf_op jit(solution)/shard_map/all_to_all | solution.py:176
  176.1 70.3 %copy-start.6 = (f32[3,64]{1,0:T(4,128)S(1)}, f32[3,64]{1,0:T(4,128)}, u32[]{:S(2)}) copy-start(f32[3,64]{1,0:T(4,128)} %copy-done.5) | copy-start | bytes 2308
  188.1 26.7 %all-to-all-start.6 = ((bf16[32,1,2,2048]{3,2,1,0:T(2,128)(2,1)}), bf16[32,1,2,2048]{3,2,1,0:T(2,128)(2,1)S(1)}, u32[]{:S(2)}, u32[]{:S(2)}) async-start(bf16[32,1,2,2048]{3,2,1,0:T(2,128)(2,1)} %bitcast.16), calls=%async_computation.6 | async-start | bytes 524288 | tf_op jit(solution)/shard_map/all_to_all | solution.py:196
  214.8 26.7 %all-to-all-start.8 = ((bf16[32,3,1024]{2,1,0:T(4,128)(2,1)}), bf16[32,3,1024]{2,1,0:T(4,128)(2,1)S(1)}, u32[]{:S(2)}, u32[]{:S(2)}) async-start(bf16[32,3,1024]{2,1,0:T(4,128)(2,1)} %pad_maximum_fusion), calls=%async_computation.8 | async-start | bytes 524288 | tf_op jit(solution)/shard_map/all_to_all | solution.py:58
  241.6 26.7 %all-to-all-start.7 = ((bf16[32,1,2,2048]{3,2,1,0:T(2,128)(2,1)}), bf16[32,1,2,2048]{3,2,1,0:T(2,128)(2,1)S(1)}, u32[]{:S(2)}, u32[]{:S(2)}) async-start(bf16[32,1,2,2048]{3,2,1,0:T(2,128)(2,1)} %bitcast.20), calls=%async_computation.7 | async-start | bytes 524288 | tf_op jit(solution)/shard_map/all_to_all | solution.py:200
  246.4 7.0 %copy-start.8 = (f32[2048]{0:T(1024)S(1)}, f32[2048]{0:T(1024)}, u32[]{:S(2)}) copy-start(f32[2048]{0:T(1024)} %param.43) | copy-start | bytes 24580
  246.4 7.0 %copy-start.12 = (bf16[2048,32]{0,1:T(8,128)(2,1)S(1)}, bf16[2048,32]{0,1:T(8,128)(2,1)}, u32[]{:S(2)}) copy-start(bf16[2048,32]{0,1:T(8,128)(2,1)} %param.44) | copy-start | bytes 393220
  246.4 8.2 %copy-start.2 = (s32[3,6]{1,0:T(4,128)S(1)}, s32[3,6]{1,0:T(4,128)}, u32[]{:S(2)}) copy-start(s32[3,6]{1,0:T(4,128)} %param.45) | copy-start | bytes 220
  246.4 22.8 %copy-start.10 = (pred[3,6]{1,0:T(4,128)(4,1)S(1)}, pred[3,6]{1,0:T(4,128)(4,1)}, u32[]{:S(2)}) copy-start(pred[3,6]{1,0:T(4,128)(4,1)} %get-tuple-element.3) | copy-start | bytes 58
where the time goes:
time: 274 us; the launch traced here: 272 us
  waiting for transfers between devices  122 us (45%)
  starting transfers between devices  57.2 us (21%)
  blocking collectives  31.8 us (12%)
  matrix products  23 us (8%)
  other arithmetic  18.6 us (7%)
  local copies, waits for them, and re-layouts  17.8 us (6%)
    all_gather x2, blocking collectives, all_blocks(): pieces = lax.all_gather(pieces, axes[k])  31.8 us
    all_to_all x1, waiting for transfers between devices, from_everyone(): lax.all_to_all(jnp.broadcast_to(shard[None], (count, *shard.shape)), axis...  23.9 us
    all_to_all x1, waiting for transfers between devices, shards(): lax.all_to_all(outbound, EP, split_axis=0, concat_axis=0, tiled=True)  20.2 us
    dot_general x13, matrix products, matmul(): return jnp.dot(left, right, preferred_element_type=jnp.float32)  18.3 us
    all_to_all x1, starting transfers between devices, from_everyone(): lax.all_to_all(jnp.broadcast_to(shard[None], (count, *shard.shape)), axis...  17.8 us
    all_to_all x1, waiting for transfers between devices, summed_on_arrival(): lax.all_to_all(pieces, axis, split_axis=0, concat_axis=0, tiled=True)  16.4 us
    all_to_all x1, waiting for transfers between devices, shards(): lax.all_to_all(jnp.stack(results, axis=1), EP, split_axis=0, concat_axis=...  13.4 us
    all_to_all x1, waiting for transfers between devices, shards(): lax.all_to_all(input_part, EP, split_axis=0, concat_axis=1, tiled=True)  11.8 us
  transfers between devices with their start and end apart: 9, of which 9 were waited for; matrix products, arithmetic and copies ran while one was open for 13% of the time, Pallas kernels for 0%

commit v1 on v0

v1 whole, which is shorter than its diff:
```python
import functools
import types

import jax
import jax.numpy as jnp
from jax import lax
from jax.experimental import pallas as pl
from jax.experimental.pallas import tpu as pltpu
from jax.sharding import PartitionSpec as P


MESH = pl.DeviceIdType.MESH
GRP_EP = ("grp", "ep")
F32, BF16 = jnp.float32, jnp.bfloat16
GROUPS, STATE, HEAD = 8, 128, 64
EPS = 1e-06
ROUTED_SCALE = 2.5

LEGS_HIDDEN = (8,)
LEGS_GATED = (4, 4)
LEGS_RESID = (8,)


def dot(a, b):
    return jnp.dot(a, b, preferred_element_type=F32)


def dot_nt(a, b):
    return lax.dot_general(a, b, (((1,), (1,)), ((), ())), preferred_element_type=F32)


def silu(v):
    return v * (1.0 / (1.0 + jnp.exp(-v)))


def lanes(tiles):
    return jnp.concatenate(tiles, axis=1)


def kernel(nz, rows, names, *refs):
    R = types.SimpleNamespace(**dict(zip(names, refs)))
    ep = lax.axis_index("ep")
    z, c = lax.div(ep, 2), lax.rem(ep, 2)
    half = nz // 2
    mine = rows * nz

    def ring(v):
        return lax.rem(v + nz, nz)

    def peer(zz):
        return {"ep": 2 * zz + c}

    partner = {"ep": 2 * z + 1 - c}

    barrier = pltpu.get_barrier_semaphore()

    def greet(d, _):
        pl.semaphore_signal(barrier, inc=1, device_id=peer(ring(z + d)), device_id_type=MESH)
        return 0

    lax.fori_loop(1, nz, greet, 0)
    pl.semaphore_signal(barrier, inc=1, device_id=partner, device_id_type=MESH)

    load_sem = R.load_sem
    handles = []

    def load(src, dst):
        copy = pltpu.make_async_copy(src, dst, load_sem.at[len(handles)])
        copy.start()
        handles.append(copy)
        return copy

    def ready(*copies):
        for copy in copies:
            copy.wait()

    L = types.SimpleNamespace()
    L.hidden = load(R.hidden, R.v_hidden)
    L.mgain = load(R.mgain, R.v_mgain)
    L.step_w = load(R.step_w, R.v_step_w)
    L.step_b = load(R.step_b, R.v_step_b)
    L.dlog = load(R.dlog, R.v_dlog)
    L.dshift = load(R.dshift, R.v_dshift)
    L.skip = load(R.skip, R.v_skip)
    L.ids = load(R.ids, R.v_ids)
    L.taps = load(R.taps, R.v_taps)
    L.cbias = load(R.cbias, R.v_cbias)
    L.window = load(R.window, R.v_window)
    L.ggain = load(R.ggain, R.v_ggain)
    L.fgain = load(R.fgain, R.v_fgain)
    L.gate = load(R.gate, R.wg.at[c])
    L.input = load(R.input, R.wi.at[c])
    L.write = load(R.write, R.wwr.at[c])
    L.read = load(R.read, R.wwr.at[2 + c])
    L.state = load(R.state, R.o_state)
    L.out_w = load(R.out_w, R.wo.at[c])
    L.router = load(R.router, R.v_router)
    L.s_gate = load(R.s_gate, R.sg.at[c])
    L.s_up = load(R.s_up, R.su.at[c])
    L.e_gate = load(R.e_gate.at[0], R.eg.at[c])
    L.e_up = load(R.e_up.at[0], R.eu.at[c])
    L.e_down = load(R.e_down.at[0], R.ed.at[c])
    L.s_down = load(R.s_down, R.v_s_down)

    S = types.SimpleNamespace()
    swapped = []

    def swap(src, dst):
        i = len(swapped)
        copy = pltpu.make_async_remote_copy(
            src_ref=src, dst_ref=dst, send_sem=R.swap_s.at[i], recv_sem=R.swap_r.at[i], device_id=partner, device_id_type=MESH
        )
        copy.start()
        swapped.append(copy)
        return copy

    def send(src, dst, ssem, rsem, zz):
        pltpu.make_async_remote_copy(
            src_ref=src, dst_ref=dst, send_sem=ssem, recv_sem=rsem, device_id=peer(zz), device_id_type=MESH
        ).start()

    def wait_recv(dst, ssem, rsem):
        pltpu.make_async_remote_copy(
            src_ref=dst, dst_ref=dst, send_sem=ssem, recv_sem=rsem, device_id=partner, device_id_type=MESH
        ).wait_recv()

    def wait_send(src, ssem, rsem):
        pltpu.make_async_remote_copy(
            src_ref=src, dst_ref=src, send_sem=ssem, recv_sem=rsem, device_id=partner, device_id_type=MESH
        ).wait_send()

    class Gather:
        def __init__(self, buf, ssem, rsem, legs):
            self.buf, self.ssem, self.rsem, self.legs, self.count = buf, ssem, rsem, legs, 0

        def one(self, block, zz):
            send(self.buf.at[block], self.buf.at[block], self.ssem.at[self.count], self.rsem.at[block], zz)
            self.count += 1

        def leg(self, done, length, block_of):
            for j in range(length, 0, -1):
                if done + j == half:
                    turn = 1 - 2 * c
                    self.one(block_of(turn), ring(z + turn * j))
                else:
                    for sign in (1, -1):
                        self.one(block_of(sign), ring(z + sign * j))

        def start(self):
            self.leg(0, self.legs[0], lambda sign: z)

        def finish(self, arrived):
            buf, done, seen = self.buf, self.legs[0], []

            def await_block(src):
                wait_recv(buf.at[src], self.ssem.at[0], self.rsem.at[src])

            for length in self.legs[1:]:
                for sign in (1, -1):
                    await_block(ring(z - sign * done))
                seen.append(done)
                at = done
                self.leg(done, length, lambda sign: ring(z - sign * at))
                done += length
            for distance in range(1, half + 1):
                for sign in (1, -1) if distance < half else (1,):
                    src = ring(z - sign * distance)
                    if distance not in seen:
                        await_block(src)
                    arrived(src)

        def drain(self):
            for i in range(self.count):
                wait_send(self.buf.at[0], self.ssem.at[i], self.rsem.at[0])

    def exchange(out, into, ssem, rsem):
        def body(i, _):
            k = lax.div(i + 1, 2)
            d = half + jnp.where(lax.rem(i, 2) == 1, -k, k)
            zz = ring(z + d)
            send(out.at[zz], into.at[z], ssem.at[i], rsem.at[z], zz)
            return 0

        lax.fori_loop(0, nz - 1, body, 0)
        into[z] = out[z]

    def collect(into, ssem, rsem, arrived, init=0):
        def body(d, carry):
            src = ring(z + d)
            wait_recv(into.at[src], ssem.at[0], rsem.at[src])
            return arrived(src, carry)

        return lax.fori_loop(1, nz, body, init)

    def drain(out, ssem, rsem):
        def body(i, _):
            wait_send(out.at[0], ssem.at[i], rsem.at[0])
            return 0

        lax.fori_loop(0, nz - 1, body, 0)

    ready(L.hidden, L.mgain)
    hid = R.v_hidden[...].astype(F32)
    depth = hid.shape[1]
    dt = depth // 128
    t1 = R.t1
    for s in range(dt):
        t1[pl.ds(s, rows, stride=dt), :] = hid[:, s * 128 : (s + 1) * 128]
    hbuf = R.hbuf
    hbuf[z] = t1[...].astype(BF16)
    pl.semaphore_wait(barrier, nz)
    g_hidden = Gather(hbuf, R.h_s, R.h_r, LEGS_HIDDEN)
    g_hidden.start()
    S.gate = swap(R.gate, R.wg.at[c])
    S.input = swap(R.input, R.wi.at[c])
    S.write = swap(R.write, R.wwr.at[c])
    S.read = swap(R.read, R.wwr.at[2 + c])
    S.out_w = swap(R.out_w, R.wo.at[c])
    S.s_gate = swap(R.s_gate, R.sg.at[c])
    S.s_up = swap(R.s_up, R.su.at[c])

    mgain = R.v_mgain[...]
    mrow = lanes([mgain[s : s + 1, :] for s in range(dt)])
    scale = lax.rsqrt(jnp.mean(hid * hid, axis=1, keepdims=True) + EPS)
    normed = (hid * scale * mrow).astype(BF16)
    ready(L.step_w, L.step_b, L.dlog, L.dshift, L.skip, L.ids, L.taps, L.cbias, L.window, L.ggain, L.fgain)
    pre = dot_nt(normed, R.v_step_w[...]) + R.v_step_b[...]
    step = jnp.maximum(pre, 0.0) + jnp.log1p(jnp.exp(-jnp.abs(pre)))
    decay = jnp.exp(R.v_dshift[...] - step * jnp.exp(R.v_dlog[...]))
    heads = decay.shape[1]
    t2 = R.t2
    t2[...] = jnp.zeros_like(t2)
    t2[0:rows, :] = decay
    t2[rows : 2 * rows, :] = step
    t2[2 * rows : 2 * rows + 1, :] = R.v_skip[...]
    per_head = t2[...]
    p_hi = per_head.astype(BF16)
    p_rest = per_head - p_hi.astype(F32)
    p_mid = p_rest.astype(BF16)
    p_lo = (p_rest - p_mid.astype(F32)).astype(BF16)
    span = heads // GROUPS * HEAD
    ex = R.ex
    for g in range(GROUPS):
        head_of = g * (heads // GROUPS) + lax.div(lax.broadcasted_iota(jnp.int32, (heads, span), 1), HEAD)
        spread = (head_of == lax.broadcasted_iota(jnp.int32, (heads, span), 0)).astype(F32).astype(BF16)
        ex[:, g * span : (g + 1) * span] = dot(p_hi, spread) + dot(p_mid, spread) + dot(p_lo, spread)
    eye = lax.broadcasted_iota(jnp.int32, (heads, heads), 0) == lax.broadcasted_iota(jnp.int32, (heads, heads), 1)
    for b in range(rows):
        column = jnp.sum(jnp.where(eye, decay[b : b + 1, :], 0.0), axis=1, keepdims=True)
        R.dcol[b] = jnp.broadcast_to(column, (heads, STATE))

    taps = R.v_taps[...].astype(F32)
    conv = R.conv
    for b in range(rows):
        past = R.v_window[b].astype(F32)
        conv[b : b + 1, :] = jnp.sum(past * taps[0:3, :], axis=0, keepdims=True) + R.v_cbias[...]
        R.nwf[b, 0:2, :] = past[1:3, :]

    ids = R.v_ids[...]
    lane3 = lax.broadcasted_iota(jnp.int32, (rows, 128), 1)
    slot3 = lax.broadcasted_iota(jnp.int32, (rows, 128), 0) * 32
    named = jnp.zeros((rows, 128), F32)
    for k in range(ids.shape[1]):
        named = named + jnp.where(lane3 == ids[:, k : k + 1] + slot3, 1.0, 0.0)
    named = jnp.sum(named, axis=0, keepdims=True)

    ready(L.state)
    o_state, sbf = R.o_state, R.sbf
    tiles = heads * HEAD // 128

    def cast_state(i, _):
        sbf[i] = o_state[i].astype(BF16)
        return 0

    lax.fori_loop(0, rows * tiles, cast_state, 0)

    f1 = R.f1

    def spread_hidden(src):
        for j in range(rows):
            at = pl.multiple_of(src * (rows * 24) + j * 24, 8)
            f1[pl.ds(at, dt), :] = hbuf[src, j * dt : (j + 1) * dt, :].astype(F32)

    spread_hidden(z)
    g_hidden.finish(spread_hidden)

    xs = [f1[pl.ds(s, mine, stride=24), :] for s in range(dt)]
    hcol = jnp.zeros_like(xs[0])
    total = jnp.zeros_like(xs[0])
    for s in range(dt):
        total = total + xs[s] * xs[s]
        hcol = jnp.where(z == s, xs[s], hcol)
    R.hcol[...] = hcol
    scale = lax.rsqrt(jnp.sum(total, axis=1, keepdims=True) / depth + EPS)
    x = R.x
    for s in range(dt):
        x[:, s * 128 : (s + 1) * 128] = (xs[s] * scale * mgain[s : s + 1, :]).astype(BF16)

    ready(L.gate, L.input, L.write, L.read)
    ready(S.gate, S.input, S.write, S.read)
    nx = x[...]
    prj = R.prj
    gates = dot(nx, lanes([R.wg[0], R.wg[1]]))
    inputs = dot(nx, lanes([R.wi[0], R.wi[1]]))
    prj[0], prj[1] = gates[:, :128], gates[:, 128:]
    prj[2], prj[3] = inputs[:, :128], inputs[:, 128:]
    wwr = R.wwr[...]
    prj[4] = dot_nt(nx, wwr.reshape(wwr.shape[0] * wwr.shape[1], wwr.shape[2]))
    m = R.m
    for t in range(5):
        for j in range(rows):
            m[pl.ds(3 * t + j, nz, stride=16), :] = prj[t, pl.ds(j, nz, stride=rows), :]
    m[pl.ds(15, nz, stride=16), :] = jnp.broadcast_to(named, (nz, 128))
    pout, pin = R.pout, R.pin
    for r in range(nz):
        pout[r] = m[16 * r : 16 * (r + 1), :].astype(BF16)
    exchange(pout, pin, R.p_s, R.p_r)
    S.e_gate = swap(R.e_gate.at[0], R.eg.at[c])
    S.e_up = swap(R.e_up.at[0], R.eu.at[c])
    S.e_down = swap(R.e_down.at[0], R.ed.at[c])
    g_hidden.drain()

    def spread_proj(src, carry):
        m[pl.ds(pl.multiple_of(src * 16, 16), 16), :] = pin[src].astype(F32)
        return carry

    spread_proj(z, 0)
    collect(pin, R.p_s, R.p_r, spread_proj)

    def tile(zz, t):
        return m[pl.ds(16 * zz + 3 * t, rows), :]

    gate_rows = lanes([tile(zz, t) for zz in range(nz) for t in (0, 1)])
    wr = [tile(zz, 4) for zz in range(nz)]
    low = lax.broadcasted_iota(jnp.int32, (rows, 128), 1) < 64
    rolled = [pltpu.roll(v, 64, 1) for v in wr]
    writes = [jnp.where(low, wr[2 * g], rolled[2 * g + 1]) for g in range(GROUPS)]
    reads = [jnp.where(low, rolled[2 * g], wr[2 * g + 1]) for g in range(GROUPS)]
    fresh = lanes([tile(zz, t) for zz in range(nz) for t in (2, 3)] + writes + reads)
    convolved = silu(conv[...] + fresh * taps[3:4, :])
    inner = heads * HEAD
    head_in = convolved[:, :inner]
    write = convolved[:, inner : inner + GROUPS * STATE]
    read = convolved[:, inner + GROUPS * STATE :]
    row_of = lax.broadcasted_iota(jnp.int32, (rows, STATE), 0)
    gated = []
    for g in range(GROUPS):
        rd = read[:, g * STATE : (g + 1) * STATE]
        wt = write[:, g * STATE : (g + 1) * STATE]
        acc = jnp.zeros((rows, span), F32)
        for b in range(rows):
            lhs = jnp.where(row_of == b, rd, 0.0).astype(BF16)
            first = (b * tiles) + g * (span // 128)
            held = sbf[first : first + span // 128]
            acc = acc + dot_nt(lhs, held.reshape(span, STATE))
        cut = slice(g * span, (g + 1) * span)
        hg = head_in[:, cut]
        inner_dot = jnp.sum(rd * wt, axis=1, keepdims=True)
        mixed = ex[0:rows, cut] * acc + (ex[rows : 2 * rows, cut] * inner_dot + ex[2 * rows : 2 * rows + 1, cut]) * hg
        mixed = mixed.astype(BF16).astype(F32) * silu(gate_rows[:, cut])
        mixed = mixed * lax.rsqrt(jnp.mean(mixed * mixed, axis=1, keepdims=True) + EPS)
        gated.append(mixed * R.v_ggain[:, cut])
    gated = lanes(gated)
    t3 = R.t3
    gt = inner // 128
    for k in range(gt):
        t3[pl.ds(k, rows, stride=gt), :] = gated[:, k * 128 : (k + 1) * 128]
    gbuf = R.gbuf
    gbuf[z] = t3[...].astype(BF16)
    g_gated = Gather(gbuf, R.g_s, R.g_r, LEGS_GATED)
    g_gated.start()

    drain(pout, R.p_s, R.p_r)
    masks = m[pl.ds(15, nz, stride=16), :]
    member = R.member
    for j in range(rows):
        member[pl.ds(j, nz, stride=rows), :] = pltpu.roll(masks, 128 - 32 * j, 1) if j else masks
    for b in range(rows):
        R.nwf[b, 2:3, :] = fresh[b : b + 1, :]
        R.o_window[b] = R.nwf[b].astype(BF16)
    u2, w2 = R.u2, R.w2
    u = ex[rows : 2 * rows, :] * head_in
    for k in range(gt):
        u2[pl.ds(k, rows, stride=gt), :] = u[:, k * 128 : (k + 1) * 128]
    for g in range(GROUPS):
        w2[pl.ds(g, rows, stride=GROUPS), :] = write[:, g * STATE : (g + 1) * STATE]
    f3 = R.f3

    def spread_gated(src):
        for j in range(rows):
            at = pl.multiple_of(src * (rows * 40) + j * 40, 8)
            f3[pl.ds(at, gt), :] = gbuf[src, j * gt : (j + 1) * gt, :].astype(F32)

    spread_gated(z)
    g_gated.finish(spread_gated)

    ready(L.out_w)
    ready(S.out_w)
    wo = R.wo[...]
    wo = wo.reshape(wo.shape[0] * wo.shape[1], wo.shape[2])
    a = R.a
    for k in range(gt):
        a[:, k * 128 : (k + 1) * 128] = f3[pl.ds(k, mine, stride=40), :].astype(BF16)
    rbuf = R.rbuf
    part = (R.hcol[...] + dot_nt(a[...], wo)).astype(BF16)
    rbuf[z] = part
    g_resid = Gather(rbuf, R.r_s, R.r_r, LEGS_RESID)
    g_resid.start()

    ready(L.s_gate, L.s_up)
    ready(S.s_gate)
    ready(S.s_up)
    shared_in = (part.astype(F32) * R.v_fgain[pl.ds(z, 1), :]).astype(BF16)
    sg, su = R.sg[...], R.su[...]
    sg = sg.reshape(sg.shape[0] * sg.shape[1], sg.shape[2])
    su = su.reshape(su.shape[0] * su.shape[1], su.shape[2])
    units = sg.shape[1]
    ut = units // 128
    pre_g, pre_u = dot(shared_in, sg), dot(shared_in, su)
    m6 = R.m6
    for k in range(ut):
        m6[pl.ds(k, mine, stride=2 * ut), :] = pre_g[:, k * 128 : (k + 1) * 128]
        m6[pl.ds(ut + k, mine, stride=2 * ut), :] = pre_u[:, k * 128 : (k + 1) * 128]
    qout, qin = R.qout, R.qin
    block = rows * 2 * ut
    for r in range(nz):
        qout[r] = m6[block * r : block * (r + 1), :].astype(BF16)
    exchange(qout, qin, R.q_s, R.q_r)

    eye2 = lax.broadcasted_iota(jnp.int32, (128, 128), 0) == lax.broadcasted_iota(jnp.int32, (128, 128), 1)

    def next_state(i, _):
        b, k = lax.div(i, tiles), lax.rem(i, tiles)
        column = jnp.sum(jnp.where(eye2, u2[pl.ds(i, 1), :], 0.0), axis=1, keepdims=True)
        fresh_part = column * w2[pl.ds(b * GROUPS + lax.div(k, tiles // GROUPS), 1), :]
        for hh in range(128 // HEAD):
            cut = slice(hh * HEAD, (hh + 1) * HEAD)
            keep = R.dcol[b, pl.ds((128 // HEAD) * k + hh, 1), :]
            o_state[i, cut, :] = o_state[i, cut, :] * keep + fresh_part[cut, :]
        return 0

    lax.fori_loop(0, rows * tiles, next_state, 0)
    g_gated.drain()
    g_resid.finish(lambda src: None)

    fgain = R.v_fgain[...]
    total = jnp.zeros((mine, 128), F32)
    for s in range(nz):
        v = rbuf[s].astype(F32)
        total = total + v * v
    scale = lax.rsqrt(jnp.sum(total, axis=1, keepdims=True) / depth + EPS)
    for s in range(nz):
        x[:, s * 128 : (s + 1) * 128] = (rbuf[s].astype(F32) * scale * fgain[s : s + 1, :]).astype(BF16)
    ready(L.router, L.e_gate, L.e_up, L.e_down)
    rx = x[...]
    experts = R.v_router.shape[0]
    logits = dot_nt(rx, R.v_router[...])
    chosen = member[...][:, :experts] / (1.0 + jnp.exp(-logits))
    weights = ROUTED_SCALE * chosen / jnp.sum(chosen, axis=1, keepdims=True)
    lane_e = lax.broadcasted_iota(jnp.int32, (mine, experts), 1)
    ready(S.e_gate, S.e_up, S.e_down)
    unit = R.eg.shape[2]
    hid_e = R.hid_e
    w_e = []
    for e in range(2):
        w_e.append(jnp.sum(jnp.where(lane_e == 2 * z + e, weights, 0.0), axis=1, keepdims=True))
        for n in range(0, unit, 256):
            up = dot(rx, R.eu[e, :, n : n + 256])
            hid_e[e, :, n : n + 256] = (silu(dot(rx, R.eg[e, :, n : n + 256])) * up).astype(BF16)
    m5 = R.m5
    for n in range(0, depth, 256):
        both = jnp.zeros((mine, 256), F32)
        for e in range(2):
            res = dot(hid_e[e], R.ed[e, :, n : n + 256]).astype(BF16).astype(F32)
            both = both + w_e[e] * res
        for i in range(2):
            m5[pl.ds(n // 128 + i, mine, stride=24), :] = both[:, i * 128 : (i + 1) * 128]
    cout, cin = R.cout, R.cin
    for r in range(nz):
        for j in range(rows):
            at = (rows * r + j) * 24
            cout[r, j * dt : (j + 1) * dt, :] = m5[at : at + dt, :].astype(BF16)
    exchange(cout, cin, R.c_s, R.c_r)

    first = lax.broadcasted_iota(jnp.int32, (8, mine), 0) + rows * z
    pick = (first == lax.broadcasted_iota(jnp.int32, (8, mine), 1)).astype(F32).astype(BF16)
    own = lanes([dot(pick, rbuf[s]) for s in range(nz)])[0:rows, :]
    scale = lax.rsqrt(jnp.mean(own * own, axis=1, keepdims=True) + EPS)
    t6 = R.t6
    t6[...] = collect(qin, R.q_s, R.q_r, lambda src, acc: acc + qin[src].astype(F32), qin[z].astype(F32))
    pre_g = lanes([t6[pl.ds(k, rows, stride=2 * ut), :] for k in range(ut)])
    pre_u = lanes([t6[pl.ds(ut + k, rows, stride=2 * ut), :] for k in range(ut)])
    shared_hidden = (silu(scale * pre_g) * (scale * pre_u)).astype(BF16)
    ready(L.s_down)
    own = own + dot(shared_hidden, R.v_s_down[...])
    g_resid.drain()
    drain(qout, R.q_s, R.q_r)
    t1[...] = collect(cin, R.c_s, R.c_r, lambda src, acc: acc + cin[src].astype(F32), cin[z].astype(F32))
    routed = lanes([t1[pl.ds(s, rows, stride=dt), :] for s in range(dt)])
    R.o_out[...] = (own + routed).astype(BF16)
    drain(cout, R.c_s, R.c_r)


def layer(
    nz, hidden, window, state, gate, input, write, read, step_w, step_b, dlog, dshift, skip, taps, cbias, mgain, ggain, out_w, fgain,
    router, ids, e_gate, e_up, e_down, s_gate, s_up, s_down
):
    A = types.SimpleNamespace(**locals())
    del A.nz
    inputs = tuple(vars(A))
    rows, depth = A.hidden.shape
    heads = A.step_b.shape[0]
    inner = heads * HEAD
    conv_dim = A.taps.shape[1]
    pre_rows = rows * 2 * A.s_gate.shape[1] // 128
    mine = rows * nz
    dt, gt = depth // 128, inner // 128
    state_shape = A.state.shape
    A.state = A.state.reshape(rows * gt, 128, STATE)
    A.write, A.read, A.step_w, A.out_w, A.router = A.write.T, A.read.T, A.step_w.T, A.out_w.T, A.router.T
    A.mgain, A.fgain = A.mgain.reshape(dt, 128), A.fgain.reshape(dt, 128)
    A.step_b, A.dlog, A.skip = A.step_b.reshape(1, heads), A.dlog.reshape(1, heads), A.skip.reshape(1, heads)
    A.cbias, A.ggain = A.cbias.reshape(1, conv_dim), A.ggain.reshape(1, inner)

    def like(array, *lead):
        return pltpu.VMEM((*lead, *array.shape), array.dtype)

    def f32(*shape):
        return pltpu.VMEM(shape, F32)

    def bf16(*shape):
        return pltpu.VMEM(shape, BF16)

    def sems(n):
        return pltpu.SemaphoreType.DMA((n,))

    scratch = dict(
        v_hidden=like(A.hidden), v_mgain=like(A.mgain), v_step_w=like(A.step_w), v_step_b=like(A.step_b), v_dlog=like(A.dlog),
        v_dshift=like(A.dshift), v_skip=like(A.skip), v_ids=like(A.ids), v_taps=like(A.taps), v_cbias=like(A.cbias),
        v_window=like(A.window), v_ggain=like(A.ggain), v_fgain=like(A.fgain), v_router=like(A.router), v_s_down=like(A.s_down),
        wg=like(A.gate, 2), wi=like(A.input, 2), wwr=like(A.write, 4), wo=like(A.out_w, 2), sg=like(A.s_gate, 2),
        su=like(A.s_up, 2), eg=like(A.e_gate[0], 2), eu=like(A.e_up[0], 2), ed=like(A.e_down[0], 2),
        t1=f32(rows * dt, 128), t2=f32(8, heads), t3=f32(rows * gt, 128), t6=f32(pre_rows, 128), ex=f32(8, inner),
        dcol=f32(rows, heads, STATE), conv=f32(rows, conv_dim), nwf=f32(rows, 3, conv_dim),
        sbf=bf16(rows * gt, 128, STATE), f1=f32(mine * 24, 128), f3=f32(mine * 40, 128), m5=f32(mine * 24, 128),
        m6=f32(nz * pre_rows, 128), hcol=f32(mine, 128), x=bf16(mine, depth), a=bf16(mine, inner), prj=f32(5, mine, 128),
        m=f32(nz * 16, 128), member=f32(mine, 128), u2=f32(rows * gt, 128), w2=f32(rows * GROUPS, 128),
        hid_e=bf16(2, mine, A.e_gate.shape[2]),
        hbuf=bf16(nz, rows * dt, 128), gbuf=bf16(nz, rows * gt, 128), rbuf=bf16(nz, mine, 128), pout=bf16(nz, 16, 128),
        pin=bf16(nz, 16, 128), qout=bf16(nz, pre_rows, 128), qin=bf16(nz, pre_rows, 128), cout=bf16(nz, rows * dt, 128),
        cin=bf16(nz, rows * dt, 128),
        load_sem=sems(32), swap_s=sems(10), swap_r=sems(10), h_s=sems(nz), h_r=sems(nz), p_s=sems(nz), p_r=sems(nz),
        g_s=sems(nz), g_r=sems(nz), r_s=sems(nz), r_r=sems(nz), q_s=sems(nz), q_r=sems(nz), c_s=sems(nz), c_r=sems(nz),
    )
    outs = dict(o_out=like(A.hidden), o_state=like(A.state), o_window=like(A.window))
    vm, anywhere = pl.BlockSpec(memory_space=pltpu.VMEM), pl.BlockSpec(memory_space=pl.ANY)
    made = pl.pallas_call(
        functools.partial(kernel, nz, rows, inputs + tuple(outs) + tuple(scratch)),
        out_shape=tuple(outs.values()),
        in_specs=[anywhere] * len(inputs),
        out_specs=(vm,) * 3,
        scratch_shapes=list(scratch.values()),
        compiler_params=pltpu.CompilerParams(collective_id=0, has_side_effects=True, vmem_limit_bytes=48 * 1024 * 1024),
        name="layer",
    )(*[getattr(A, name) for name in inputs])
    out, state, window = pl.pallas_call(
        write_out,
        out_shape=tuple(jax.ShapeDtypeStruct(v.shape, v.dtype) for v in made),
        in_specs=[vm] * 3,
        out_specs=(anywhere,) * 3,
        scratch_shapes=[sems(2 + PIECES)],
        compiler_params=pltpu.CompilerParams(vmem_limit_bytes=2**20),
        name="store",
    )(*[pltpu.with_memory_space_constraint(v, pltpu.VMEM) for v in made])
    return out, state.reshape(state_shape), window


PIECES = 4


def write_out(x, state, window, o_x, o_state, o_window, sem):
    copies = []
    step = state.shape[0] // PIECES
    for i in range(PIECES):
        copies.append(pltpu.make_async_copy(state.at[pl.ds(i * step, step)], o_state.at[pl.ds(i * step, step)], sem.at[i]))
    copies.append(pltpu.make_async_copy(x, o_x, sem.at[PIECES]))
    copies.append(pltpu.make_async_copy(window, o_window, sem.at[PIECES + 1]))
    for copy in copies:
        copy.start()
    for copy in copies:
        copy.wait()


def solution(mesh):
    nz = mesh.shape["ep"] // 2
    rows2, rows3, rows4 = P(GRP_EP, None), P(GRP_EP, None, None), P(GRP_EP, None, None, None)
    cols, lead, lead3 = P(None, "ep"), P("ep", None), P("ep", None, None)
    return jax.shard_map(
        functools.partial(layer, nz),
        mesh=mesh,
        in_specs=(
            rows2, rows3, rows4, cols, cols, cols, cols, P(), P(), P(), rows2, P(), P(), P(), P(), P(), cols, P(), P(), rows2,
            lead3, lead3, lead3, lead, lead, P(),
        ),
        out_specs=(rows2, rows4, rows3),
        check_vma=False,
    )
```

time: 274 us -> 76.9 us (0.28)
  waiting for transfers between devices: 122 us -> 0 us
  Pallas kernels: 0 us -> 75.9 us
  starting transfers between devices: 57.2 us -> 0 us
  blocking collectives: 31.8 us -> 0 us
  matrix products: 23 us -> 0 us
  other arithmetic: 18.6 us -> 0 us
  local copies, waits for them, and re-layouts: 17.8 us -> 0 us
    all_to_all x9 -> x0, waiting for transfers between devices: 122 us -> none  [the longest x1 23.9 us: from_everyone(): lax.all_to_all(jnp.broadcast_to(shard[None], (count, *shard.shape)), axis...]
    pallas_call x0 -> x2, Pallas kernels: none -> 75.9 us  [the longest x1 73.1 us: layer(): pl.pallas_call(functools.partial(kernel, nz, rows, inputs + tuple(outs) +...]
    all_to_all x9 -> x0, starting transfers between devices: 57.2 us -> none  [the longest x1 17.8 us: from_everyone(): lax.all_to_all(jnp.broadcast_to(shard[None], (count, *shard.shape)), axis...]
    all_gather x2 -> x0, blocking collectives: 31.8 us -> none  [all_blocks(): pieces = lax.all_gather(pieces, axes[k])]
    dot_general x14 -> x0, matrix products: 23 us -> none  [the longest x13 18.3 us: matmul(): return jnp.dot(left, right, preferred_element_type=jnp.float32)]
    add x1 -> x0, other arithmetic: 6.99 us -> none  [shards(): decay_rate[..., None, None] * carried]
    all_to_all x9 -> x0, local copies, waits for them, and re-layouts: 3.43 us -> none  [the longest x3 0.76 us: shards(): lax.all_to_all(write_part, EP, split_axis=0, concat_axis=1, tiled=True)]
  transfers between devices with their start and end apart: 9 -> 0, of which waited for: 9 -> 0; matrix products, arithmetic and copies ran while one was open for 13% -> 0% of each run, Pallas kernels for 0% -> 0%
where the time goes in v1:
time: 76.9 us; the launch traced here: 76.5 us
  Pallas kernels  75.9 us (99%)
    pallas_call x1, Pallas kernels, layer(): pl.pallas_call(functools.partial(kernel, nz, rows, inputs + tuple(outs) +...  73.1 us
    pallas_call x1, Pallas kernels, layer(): pl.pallas_call(write_out, out_shape=tuple((jax.ShapeDtypeStruct(v.shape,...  2.76 us

profile of v1, /device:TPU:86, one launch (start us, length us, event | category | flops | bytes accessed | tf_op | source)
XLA Modules:
  0.0 76.5 jit_solution(12545623112341496507)
XLA Ops:
  0.6 73.1 %layer.1 = (bf16[3,2048]{1,0:T(4,128)(2,1)S(1)}, f32[96,128,128]{2,1,0:T(8,128)S(1)}, bf16[3,3,6144]{2,1,0:T(4,128)(2,1)S(1)}) custom-call(bf16[3,2048]{1,0:T(4,128)(2,1)} %refs_0_.1, bf16[3,3,6144]{2,1,0:T(4,128)(2,1)} %refs_1_.1, f32[96,128,128]{2,1,0:T(8,128)} %bitcast.14, bf16[2048,128]{1,0:T(8,128)(2,1)} %refs_3_.1, bf16[2048,128]{1,0:T(8,128)(2,1)} %refs_4_.1, ...), custom_call_target="tpu_custom_call" | custom-call | tf_op jit(solution)/shard_map/layer/pallas_call | solution.py:557
  73.8 2.8 %store.1 = (bf16[3,2048]{1,0:T(4,128)(2,1)}, f32[96,128,128]{2,1,0:T(8,128)}, bf16[3,3,6144]{2,1,0:T(4,128)(2,1)}) custom-call(bf16[3,2048]{1,0:T(4,128)(2,1)S(1)} %get-tuple-element.9.x, f32[96,128,128]{2,1,0:T(8,128)S(1)} %get-tuple-element.10.state, bf16[3,3,6144]{2,1,0:T(4,128)(2,1)S(1)} %get-tuple-element.11.window), custom_call_target="tpu_custom_call" | custom-call | tf_op jit(solution)/shard_map/store/pallas_call | solution.py:566

commit v2 on v1

--- a/solution.py
+++ b/solution.py
@@ -16,9 +16,11 @@
 EPS = 1e-06
 ROUTED_SCALE = 2.5
 
-LEGS_HIDDEN = (8,)
-LEGS_GATED = (4, 4)
-LEGS_RESID = (8,)
+LEGS_HIDDEN = ((4, 4), (4, 4))
+LEGS_GATED = ((4, 4), (2, 2, 2, 2))
+LEGS_RESID = ((4, 4), (4, 4))
+CUT_SHARED = (4, 4)
+CUT_ROUTED = (4, 4)
 
 
 def dot(a, b):
@@ -52,15 +54,6 @@
 
     partner = {"ep": 2 * z + 1 - c}
 
-    barrier = pltpu.get_barrier_semaphore()
-
-    def greet(d, _):
-        pl.semaphore_signal(barrier, inc=1, device_id=peer(ring(z + d)), device_id_type=MESH)
-        return 0
-
-    lax.fori_loop(1, nz, greet, 0)
-    pl.semaphore_signal(barrier, inc=1, device_id=partner, device_id_type=MESH)
-
     load_sem = R.load_sem
     handles = []
 
@@ -77,6 +70,196 @@
     L = types.SimpleNamespace()
     L.hidden = load(R.hidden, R.v_hidden)
     L.mgain = load(R.mgain, R.v_mgain)
+
+    def by_core(work):
+        for core in (0, 1):
+            pl.when(c == core)(functools.partial(work, core))
+
+    barrier = pltpu.get_barrier_semaphore()
+
+    def greet(d, _):
+        pl.semaphore_signal(barrier, inc=1, device_id=peer(ring(z + d)), device_id_type=MESH)
+        pl.semaphore_signal(barrier, inc=1, device_id=peer(ring(z - d)), device_id_type=MESH)
+        return 0
+
+    pl.semaphore_signal(barrier, inc=1, device_id=partner, device_id_type=MESH)
+    near = max(LEGS_HIDDEN[0][0], LEGS_HIDDEN[1][0])
+    lax.fori_loop(1, near + 1, greet, 0)
+
+    S = types.SimpleNamespace()
+    swapped = []
+
+    def swap(src, dst):
+        i = len(swapped)
+        copy = pltpu.make_async_remote_copy(
+            src_ref=src, dst_ref=dst, send_sem=R.swap_s.at[i], recv_sem=R.swap_r.at[i], device_id=partner, device_id_type=MESH
+        )
+        copy.start()
+        swapped.append(copy)
+        return copy
+
+    def send(src, dst, ssem, rsem, zz):
+        pltpu.make_async_remote_copy(
+            src_ref=src, dst_ref=dst, send_sem=ssem, recv_sem=rsem, device_id=peer(zz), device_id_type=MESH
+        ).start()
+
+    def wait_recv(dst, ssem, rsem):
+        pltpu.make_async_remote_copy(
+            src_ref=dst, dst_ref=dst, send_sem=ssem, recv_sem=rsem, device_id=partner, device_id_type=MESH
+        ).wait_recv()
+
+    def wait_send(src, ssem, rsem):
+        pltpu.make_async_remote_copy(
+            src_ref=src, dst_ref=src, send_sem=ssem, recv_sem=rsem, device_id=partner, device_id_type=MESH
+        ).wait_send()
+
+    class Gather:
+        def __init__(self, buf, ssem, rsem, legs, each):
+            self.buf, self.ssem, self.rsem, self.legs, self.each = buf, ssem, rsem, legs, each
+            self.last = rsem.shape[0] - 1
+
+        def passed(self, core):
+            legs = self.legs[core]
+            return [sum(legs[: i + 1]) for i in range(len(legs) - 1)]
+
+        def sem(self, core, sign, distance):
+            if self.each:
+                at = 2 * (distance - 1) + (sign < 0 and distance < half)
+            elif distance in self.passed(core):
+                at = 2 * self.passed(core).index(distance) + (sign < 0)
+            else:
+                at = self.last
+            return self.rsem.at[at]
+
+        def leg(self, core, done, length, block_of):
+            for j in range(length, 0, -1):
+                for sign in (1, -1) if done + j < half else (1 - 2 * core,):
+                    block = block_of(sign)
+                    to = self.buf.at[block]
+                    send(to, to, self.ssem, self.sem(core, sign, done + j), ring(z + sign * j))
+
+        def await_block(self, core, sign, distance):
+            to = self.buf.at[ring(z - sign * distance)]
+            wait_recv(to, self.ssem, self.sem(core, sign, distance))
+
+        def start(self):
+            by_core(lambda core: self.leg(core, 0, self.legs[core][0], lambda sign: z))
+
+        def relay(self):
+            def work(core):
+                done = self.legs[core][0]
+                for length in self.legs[core][1:]:
+                    for sign in (1, -1):
+                        self.await_block(core, sign, done)
+                    self.leg(core, done, length, lambda sign: ring(z - sign * done))
+                    done += length
+
+            by_core(work)
+
+        def finish(self):
+            def work(core):
+                rest = self.buf.at[pl.ds(0, nz - 1 - 2 * len(self.passed(core)))]
+                wait_recv(rest, self.ssem, self.rsem.at[self.last])
+
+            by_core(work)
+
+        def drain(self):
+            wait_send(self.buf.at[pl.ds(0, nz - 1)], self.ssem, self.rsem.at[0])
+
+    def exchange(out, into, ssem, rsem):
+        def body(i, _):
+            k = lax.div(i + 1, 2)
+            d = half + jnp.where(lax.rem(i, 2) == 1, -k, k)
+            zz = ring(z + d)
+            send(out.at[zz], into.at[z], ssem, rsem, zz)
+            return 0
+
+        lax.fori_loop(0, nz - 1, body, 0)
+
+    def collect(into, ssem, rsem):
+        wait_recv(into.at[pl.ds(0, nz - 1)], ssem, rsem)
+
+    def drain(out, ssem, rsem):
+        wait_send(out.at[pl.ds(0, nz - 1)], ssem, rsem)
+
+    class Reduce:
+        def __init__(self, out, mid, fin, sems, cuts):
+            self.out, self.mid, self.fin, self.cuts = out, mid, fin, cuts
+            self.ssem, self.fsem, self.msem = sems.at[0], sems.at[1], (sems.at[2], sems.at[3])
+
+        def far(self, core, sign):
+            cut = self.cuts[core]
+            return half - cut - (sign != 1 - 2 * core)
+
+        def slot(self, sign, j):
+            return (half if sign < 0 else 0) + j - 1
+
+        def start(self):
+            def work(core):
+                cut = self.cuts[core]
+                if not cut:
+                    exchange(self.out, self.fin, self.ssem, self.fsem)
+                    return
+                for j in range(half - cut, 0, -1):
+                    for sign in (1, -1):
+                        if j <= self.far(core, sign):
+                            at = self.slot(sign, j)
+                            src = self.out.at[ring(z + sign * (cut + j))]
+                            send(src, self.mid.at[at], self.ssem, self.msem[sign < 0], ring(z + sign * j))
+                for j in range(cut - 1, 0, -1):
+                    for sign in (1, -1):
+                        zz = ring(z + sign * j)
+                        send(self.out.at[zz], self.fin.at[self.slot(sign, j)], self.ssem, self.fsem, zz)
+
+            by_core(work)
+
+        def relay(self):
+            def work(core):
+                cut = self.cuts[core]
+                if not cut:
+                    return
+                for sign in (1, -1):
+                    zz, many = ring(z + sign * cut), self.far(core, sign)
+                    wait_recv(self.mid.at[pl.ds(self.slot(sign, 1), many)], self.ssem, self.msem[sign < 0])
+                    terms = self.out[zz].astype(F32)
+                    for j in range(1, many + 1):
+                        terms = terms + self.mid[self.slot(sign, j)].astype(F32)
+                    self.out[zz] = terms.astype(BF16)
+                    send(self.out.at[zz], self.fin.at[self.slot(sign, cut)], self.ssem, self.fsem, zz)
+
+            by_core(work)
+
+        def finish(self, into):
+            def work(core):
+                cut = self.cuts[core]
+                total = self.out[z].astype(F32)
+                if cut:
+                    wait_recv(self.fin.at[pl.ds(0, 2 * cut)], self.ssem, self.fsem)
+                    for j in range(1, cut + 1):
+                        for sign in (1, -1):
+                            total = total + self.fin[self.slot(sign, j)].astype(F32)
+                    into[...] = total
+                else:
+                    collect(self.fin, self.ssem, self.fsem)
+                    into[...] = lax.fori_loop(1, nz, lambda d, acc: acc + self.fin[ring(z + d)].astype(F32), total)
+
+            by_core(work)
+
+        def drain(self):
+            drain(self.out, self.ssem, self.fsem)
+
+    ready(L.hidden, L.mgain)
+    hid = R.v_hidden[...].astype(F32)
+    depth = hid.shape[1]
+    dt = depth // 128
+    t1 = R.t1
+    for s in range(dt):
+        t1[pl.ds(s, rows, stride=dt), :] = hid[:, s * 128 : (s + 1) * 128]
+    hbuf = R.hbuf
+    hbuf[z] = t1[...].astype(BF16)
+    pl.semaphore_wait(barrier, 2 * near + 1)
+    g_hidden = Gather(hbuf, R.one.at[0], R.h_r, LEGS_HIDDEN, False)
+    g_hidden.start()
     L.step_w = load(R.step_w, R.v_step_w)
     L.step_b = load(R.step_b, R.v_step_b)
     L.dlog = load(R.dlog, R.v_dlog)
@@ -101,116 +284,6 @@
     L.e_up = load(R.e_up.at[0], R.eu.at[c])
     L.e_down = load(R.e_down.at[0], R.ed.at[c])
     L.s_down = load(R.s_down, R.v_s_down)
-
-    S = types.SimpleNamespace()
-    swapped = []
-
-    def swap(src, dst):
-        i = len(swapped)
-        copy = pltpu.make_async_remote_copy(
-            src_ref=src, dst_ref=dst, send_sem=R.swap_s.at[i], recv_sem=R.swap_r.at[i], device_id=partner, device_id_type=MESH
-        )
-        copy.start()
-        swapped.append(copy)
-        return copy
-
-    def send(src, dst, ssem, rsem, zz):
-        pltpu.make_async_remote_copy(
-            src_ref=src, dst_ref=dst, send_sem=ssem, recv_sem=rsem, device_id=peer(zz), device_id_type=MESH
-        ).start()
-
-    def wait_recv(dst, ssem, rsem):
-        pltpu.make_async_remote_copy(
-            src_ref=dst, dst_ref=dst, send_sem=ssem, recv_sem=rsem, device_id=partner, device_id_type=MESH
-        ).wait_recv()
-
-    def wait_send(src, ssem, rsem):
-        pltpu.make_async_remote_copy(
-            src_ref=src, dst_ref=src, send_sem=ssem, recv_sem=rsem, device_id=partner, device_id_type=MESH
-        ).wait_send()
-
-    class Gather:
-        def __init__(self, buf, ssem, rsem, legs):
-            self.buf, self.ssem, self.rsem, self.legs, self.count = buf, ssem, rsem, legs, 0
-
-        def one(self, block, zz):
-            send(self.buf.at[block], self.buf.at[block], self.ssem.at[self.count], self.rsem.at[block], zz)
-            self.count += 1
-
-        def leg(self, done, length, block_of):
-            for j in range(length, 0, -1):
-                if done + j == half:
-                    turn = 1 - 2 * c
-                    self.one(block_of(turn), ring(z + turn * j))
-                else:
-                    for sign in (1, -1):
-                        self.one(block_of(sign), ring(z + sign * j))
-
-        def start(self):
-            self.leg(0, self.legs[0], lambda sign: z)
-
-        def finish(self, arrived):
-            buf, done, seen = self.buf, self.legs[0], []
-
-            def await_block(src):
-                wait_recv(buf.at[src], self.ssem.at[0], self.rsem.at[src])
-
-            for length in self.legs[1:]:
-                for sign in (1, -1):
-                    await_block(ring(z - sign * done))
-                seen.append(done)
-                at = done
-                self.leg(done, length, lambda sign: ring(z - sign * at))
-                done += length
-            for distance in range(1, half + 1):
-                for sign in (1, -1) if distance < half else (1,):
-                    src = ring(z - sign * distance)
-                    if distance not in seen:
-                        await_block(src)
-                    arrived(src)
-
-        def drain(self):
-            for i in range(self.count):
-                wait_send(self.buf.at[0], self.ssem.at[i], self.rsem.at[0])
-
-    def exchange(out, into, ssem, rsem):
-        def body(i, _):
-            k = lax.div(i + 1, 2)
-            d = half + jnp.where(lax.rem(i, 2) == 1, -k, k)
-            zz = ring(z + d)
-            send(out.at[zz], into.at[z], ssem.at[i], rsem.at[z], zz)
-            return 0
-
-        lax.fori_loop(0, nz - 1, body, 0)
-        into[z] = out[z]
-
-    def collect(into, ssem, rsem, arrived, init=0):
-        def body(d, carry):
-            src = ring(z + d)
-            wait_recv(into.at[src], ssem.at[0], rsem.at[src])
-            return arrived(src, carry)
-
-        return lax.fori_loop(1, nz, body, init)
-
-    def drain(out, ssem, rsem):
-        def body(i, _):
-            wait_send(out.at[0], ssem.at[i], rsem.at[0])
-            return 0
-
-        lax.fori_loop(0, nz - 1, body, 0)
-
-    ready(L.hidden, L.mgain)
-    hid = R.v_hidden[...].astype(F32)
-    depth = hid.shape[1]
-    dt = depth // 128
-    t1 = R.t1
-    for s in range(dt):
-        t1[pl.ds(s, rows, stride=dt), :] = hid[:, s * 128 : (s + 1) * 128]
-    hbuf = R.hbuf
-    hbuf[z] = t1[...].astype(BF16)
-    pl.semaphore_wait(barrier, nz)
-    g_hidden = Gather(hbuf, R.h_s, R.h_r, LEGS_HIDDEN)
-    g_hidden.start()
     S.gate = swap(R.gate, R.wg.at[c])
     S.input = swap(R.input, R.wi.at[c])
     S.write = swap(R.write, R.wwr.at[c])
@@ -249,6 +322,8 @@
         column = jnp.sum(jnp.where(eye, decay[b : b + 1, :], 0.0), axis=1, keepdims=True)
         R.dcol[b] = jnp.broadcast_to(column, (heads, STATE))
 
+    g_hidden.relay()
+
     taps = R.v_taps[...].astype(F32)
     conv = R.conv
     for b in range(rows):
@@ -278,11 +353,12 @@
 
     def spread_hidden(src):
         for j in range(rows):
-            at = pl.multiple_of(src * (rows * 24) + j * 24, 8)
+            at = src * (rows * 24) + j * 24
             f1[pl.ds(at, dt), :] = hbuf[src, j * dt : (j + 1) * dt, :].astype(F32)
 
-    spread_hidden(z)
-    g_hidden.finish(spread_hidden)
+    g_hidden.finish()
+    for src in range(nz):
+        spread_hidden(src)
 
     xs = [f1[pl.ds(s, mine, stride=24), :] for s in range(dt)]
     hcol = jnp.zeros_like(xs[0])
@@ -314,18 +390,16 @@
     pout, pin = R.pout, R.pin
     for r in range(nz):
         pout[r] = m[16 * r : 16 * (r + 1), :].astype(BF16)
-    exchange(pout, pin, R.p_s, R.p_r)
+    exchange(pout, pin, R.one.at[3], R.one.at[4])
+    pin[z] = pout[z]
     S.e_gate = swap(R.e_gate.at[0], R.eg.at[c])
     S.e_up = swap(R.e_up.at[0], R.eu.at[c])
     S.e_down = swap(R.e_down.at[0], R.ed.at[c])
     g_hidden.drain()
 
-    def spread_proj(src, carry):
-        m[pl.ds(pl.multiple_of(src * 16, 16), 16), :] = pin[src].astype(F32)
-        return carry
-
-    spread_proj(z, 0)
-    collect(pin, R.p_s, R.p_r, spread_proj)
+    collect(pin, R.one.at[3], R.one.at[4])
+    for src in range(nz):
+        m[src * 16 : (src + 1) * 16, :] = pin[src].astype(F32)
 
     def tile(zz, t):
         return m[pl.ds(16 * zz + 3 * t, rows), :]
@@ -367,10 +441,11 @@
         t3[pl.ds(k, rows, stride=gt), :] = gated[:, k * 128 : (k + 1) * 128]
     gbuf = R.gbuf
     gbuf[z] = t3[...].astype(BF16)
-    g_gated = Gather(gbuf, R.g_s, R.g_r, LEGS_GATED)
+    g_gated = Gather(gbuf, R.one.at[1], R.g_r, LEGS_GATED, False)
     g_gated.start()
-
-    drain(pout, R.p_s, R.p_r)
+    g_gated.relay()
+
+    drain(pout, R.one.at[3], R.one.at[4])
     masks = m[pl.ds(15, nz, stride=16), :]
     member = R.member
     for j in range(rows):
@@ -384,15 +459,45 @@
         u2[pl.ds(k, rows, stride=gt), :] = u[:, k * 128 : (k + 1) * 128]
     for g in range(GROUPS):
         w2[pl.ds(g, rows, stride=GROUPS), :] = write[:, g * STATE : (g + 1) * STATE]
+    lane_t = lax.rem(lax.broadcasted_iota(jnp.int32, (1, 128), 1), tiles)
+
+    def advance(b):
+        u_b = u2[b * tiles : (b + 1) * tiles, :]
+        u_hi = u_b.astype(BF16).astype(F32)
+        flip = jnp.concatenate([u_hi, u_b - u_hi, u_hi, jnp.zeros((128 - 3 * tiles, 128), F32)], axis=0).T
+        R.ut[b] = flip.astype(BF16)
+        for g in range(GROUPS):
+            per = tiles // GROUPS
+            w_g = jnp.broadcast_to(w2[b * GROUPS + g : b * GROUPS + g + 1, :], (per, STATE))
+            w_hi = w_g.astype(BF16).astype(F32)
+            for part, v in enumerate((w_hi, w_hi, w_g - w_hi)):
+                R.wt[b, part * tiles + g * per : part * tiles + (g + 1) * per, :] = v
+        R.wt[b, 3 * tiles : 128, :] = jnp.zeros((128 - 3 * tiles, STATE), F32)
+        base = R.ut[b].astype(F32)
+        right = R.wt[b].astype(BF16)
+
+        def next_state(k, _, b=b, base=base, right=right):
+            fresh_part = dot(jnp.where(lane_t == k, base, 0.0).astype(BF16), right)
+            i = b * tiles + k
+            for hh in range(128 // HEAD):
+                cut = slice(hh * HEAD, (hh + 1) * HEAD)
+                keep = R.dcol[b, pl.ds((128 // HEAD) * k + hh, 1), :]
+                o_state[i, cut, :] = o_state[i, cut, :] * keep + fresh_part[cut, :]
+            return 0
+
+        lax.fori_loop(0, tiles, next_state, 0, unroll=8)
+
+    advance(0)
     f3 = R.f3
 
     def spread_gated(src):
         for j in range(rows):
-            at = pl.multiple_of(src * (rows * 40) + j * 40, 8)
+            at = src * (rows * 40) + j * 40
             f3[pl.ds(at, gt), :] = gbuf[src, j * gt : (j + 1) * gt, :].astype(F32)
 
-    spread_gated(z)
-    g_gated.finish(spread_gated)
+    g_gated.finish()
+    for src in range(nz):
+        spread_gated(src)
 
     ready(L.out_w)
     ready(S.out_w)
@@ -404,7 +509,7 @@
     rbuf = R.rbuf
     part = (R.hcol[...] + dot_nt(a[...], wo)).astype(BF16)
     rbuf[z] = part
-    g_resid = Gather(rbuf, R.r_s, R.r_r, LEGS_RESID)
+    g_resid = Gather(rbuf, R.one.at[2], R.r_r, LEGS_RESID, True)
     g_resid.start()
 
     ready(L.s_gate, L.s_up)
@@ -421,52 +526,55 @@
     for k in range(ut):
         m6[pl.ds(k, mine, stride=2 * ut), :] = pre_g[:, k * 128 : (k + 1) * 128]
         m6[pl.ds(ut + k, mine, stride=2 * ut), :] = pre_u[:, k * 128 : (k + 1) * 128]
-    qout, qin = R.qout, R.qin
+    qout = R.qout
     block = rows * 2 * ut
     for r in range(nz):
         qout[r] = m6[block * r : block * (r + 1), :].astype(BF16)
-    exchange(qout, qin, R.q_s, R.q_r)
-
-    eye2 = lax.broadcasted_iota(jnp.int32, (128, 128), 0) == lax.broadcasted_iota(jnp.int32, (128, 128), 1)
-
-    def next_state(i, _):
-        b, k = lax.div(i, tiles), lax.rem(i, tiles)
-        column = jnp.sum(jnp.where(eye2, u2[pl.ds(i, 1), :], 0.0), axis=1, keepdims=True)
-        fresh_part = column * w2[pl.ds(b * GROUPS + lax.div(k, tiles // GROUPS), 1), :]
-        for hh in range(128 // HEAD):
-            cut = slice(hh * HEAD, (hh + 1) * HEAD)
-            keep = R.dcol[b, pl.ds((128 // HEAD) * k + hh, 1), :]
-            o_state[i, cut, :] = o_state[i, cut, :] * keep + fresh_part[cut, :]
-        return 0
-
-    lax.fori_loop(0, rows * tiles, next_state, 0)
+    g_resid.relay()
+    sum_q = Reduce(qout, R.qmid, R.qfin, R.q_sem, CUT_SHARED)
+
+    for b in range(1, rows):
+        advance(b)
     g_gated.drain()
-    g_resid.finish(lambda src: None)
-
-    fgain = R.v_fgain[...]
-    total = jnp.zeros((mine, 128), F32)
-    for s in range(nz):
-        v = rbuf[s].astype(F32)
-        total = total + v * v
-    scale = lax.rsqrt(jnp.sum(total, axis=1, keepdims=True) / depth + EPS)
-    for s in range(nz):
-        x[:, s * 128 : (s + 1) * 128] = (rbuf[s].astype(F32) * scale * fgain[s : s + 1, :]).astype(BF16)
+
     ready(L.router, L.e_gate, L.e_up, L.e_down)
-    rx = x[...]
-    experts = R.v_router.shape[0]
-    logits = dot_nt(rx, R.v_router[...])
-    chosen = member[...][:, :experts] / (1.0 + jnp.exp(-logits))
+    ready(S.e_gate, S.e_up, S.e_down)
+    experts, unit = R.v_router.shape[0], R.eg.shape[2]
+    squares, logits, pre = R.squares, R.logits, R.pre
+    squares[...] = jnp.zeros_like(squares)
+    logits[...] = jnp.zeros_like(logits)
+    pre[...] = jnp.zeros_like(pre)
+
+    def features(src):
+        v = rbuf[src].astype(F32)
+        squares[...] += v * v
+        v = (v * R.v_fgain[pl.ds(src, 1), :]).astype(BF16)
+        cut = pl.ds(pl.multiple_of(src * 128, 128), 128)
+        logits[...] += dot_nt(v, R.v_router[:, cut])
+        for e in range(2):
+            pre[2 * e] += dot(v, R.eg[e, cut, :])
+            pre[2 * e + 1] += dot(v, R.eu[e, cut, :])
+
+    features(z)
+
+    def take(core):
+        for distance in range(1, half + 1):
+            for sign in (1, -1) if distance < half else (1 - 2 * core,):
+                if distance not in g_resid.passed(core):
+                    g_resid.await_block(core, sign, distance)
+                features(ring(z - sign * distance))
+
+    by_core(take)
+    sum_q.start()
+    scale = lax.rsqrt(jnp.sum(squares[...], axis=1, keepdims=True) / depth + EPS)
+    chosen = member[...][:, :experts] / (1.0 + jnp.exp(-scale * logits[...]))
     weights = ROUTED_SCALE * chosen / jnp.sum(chosen, axis=1, keepdims=True)
     lane_e = lax.broadcasted_iota(jnp.int32, (mine, experts), 1)
-    ready(S.e_gate, S.e_up, S.e_down)
-    unit = R.eg.shape[2]
     hid_e = R.hid_e
     w_e = []
     for e in range(2):
         w_e.append(jnp.sum(jnp.where(lane_e == 2 * z + e, weights, 0.0), axis=1, keepdims=True))
-        for n in range(0, unit, 256):
-            up = dot(rx, R.eu[e, :, n : n + 256])
-            hid_e[e, :, n : n + 256] = (silu(dot(rx, R.eg[e, :, n : n + 256])) * up).astype(BF16)
+        hid_e[e] = (silu(scale * pre[2 * e]) * (scale * pre[2 * e + 1])).astype(BF16)
     m5 = R.m5
     for n in range(0, depth, 256):
         both = jnp.zeros((mine, 256), F32)
@@ -475,30 +583,33 @@
             both = both + w_e[e] * res
         for i in range(2):
             m5[pl.ds(n // 128 + i, mine, stride=24), :] = both[:, i * 128 : (i + 1) * 128]
-    cout, cin = R.cout, R.cin
+    cout = R.cout
     for r in range(nz):
         for j in range(rows):
             at = (rows * r + j) * 24
             cout[r, j * dt : (j + 1) * dt, :] = m5[at : at + dt, :].astype(BF16)
-    exchange(cout, cin, R.c_s, R.c_r)
+    sum_c = Reduce(cout, R.cmid, R.cfin, R.c_sem, CUT_ROUTED)
+    sum_c.start()
+    sum_q.relay()
+    sum_c.relay()
 
     first = lax.broadcasted_iota(jnp.int32, (8, mine), 0) + rows * z
     pick = (first == lax.broadcasted_iota(jnp.int32, (8, mine), 1)).astype(F32).astype(BF16)
     own = lanes([dot(pick, rbuf[s]) for s in range(nz)])[0:rows, :]
     scale = lax.rsqrt(jnp.mean(own * own, axis=1, keepdims=True) + EPS)
     t6 = R.t6
-    t6[...] = collect(qin, R.q_s, R.q_r, lambda src, acc: acc + qin[src].astype(F32), qin[z].astype(F32))
+    sum_q.finish(t6)
     pre_g = lanes([t6[pl.ds(k, rows, stride=2 * ut), :] for k in range(ut)])
     pre_u = lanes([t6[pl.ds(ut + k, rows, stride=2 * ut), :] for k in range(ut)])
     shared_hidden = (silu(scale * pre_g) * (scale * pre_u)).astype(BF16)
     ready(L.s_down)
     own = own + dot(shared_hidden, R.v_s_down[...])
     g_resid.drain()
-    drain(qout, R.q_s, R.q_r)
-    t1[...] = collect(cin, R.c_s, R.c_r, lambda src, acc: acc + cin[src].astype(F32), cin[z].astype(F32))
+    sum_q.drain()
+    sum_c.finish(t1)
     routed = lanes([t1[pl.ds(s, rows, stride=dt), :] for s in range(dt)])
     R.o_out[...] = (own + routed).astype(BF16)
-    drain(cout, R.c_s, R.c_r)
+    sum_c.drain()
 
 
 def layer(
@@ -543,14 +654,14 @@
         t1=f32(rows * dt, 128), t2=f32(8, heads), t3=f32(rows * gt, 128), t6=f32(pre_rows, 128), ex=f32(8, inner),
         dcol=f32(rows, heads, STATE), conv=f32(rows, conv_dim), nwf=f32(rows, 3, conv_dim),
         sbf=bf16(rows * gt, 128, STATE), f1=f32(mine * 24, 128), f3=f32(mine * 40, 128), m5=f32(mine * 24, 128),
-        m6=f32(nz * pre_rows, 128), hcol=f32(mine, 128), x=bf16(mine, depth), a=bf16(mine, inner), prj=f32(5, mine, 128),
+        m6=f32(nz * pre_rows, 128), hcol=f32(mine, 128), ut=bf16(rows, 128, 128), wt=f32(rows, 128, STATE), x=bf16(mine, depth), a=bf16(mine, inner), prj=f32(5, mine, 128),
         m=f32(nz * 16, 128), member=f32(mine, 128), u2=f32(rows * gt, 128), w2=f32(rows * GROUPS, 128),
-        hid_e=bf16(2, mine, A.e_gate.shape[2]),
+        hid_e=bf16(2, mine, A.e_gate.shape[2]), squares=f32(mine, 128), logits=f32(mine, A.router.shape[0]),
+        pre=f32(4, mine, A.e_gate.shape[2]),
         hbuf=bf16(nz, rows * dt, 128), gbuf=bf16(nz, rows * gt, 128), rbuf=bf16(nz, mine, 128), pout=bf16(nz, 16, 128),
-        pin=bf16(nz, 16, 128), qout=bf16(nz, pre_rows, 128), qin=bf16(nz, pre_rows, 128), cout=bf16(nz, rows * dt, 128),
-        cin=bf16(nz, rows * dt, 128),
-        load_sem=sems(32), swap_s=sems(10), swap_r=sems(10), h_s=sems(nz), h_r=sems(nz), p_s=sems(nz), p_r=sems(nz),
-        g_s=sems(nz), g_r=sems(nz), r_s=sems(nz), r_r=sems(nz), q_s=sems(nz), q_r=sems(nz), c_s=sems(nz), c_r=sems(nz),
+        pin=bf16(nz, 16, 128), qout=bf16(nz, pre_rows, 128), qmid=bf16(nz, pre_rows, 128), qfin=bf16(nz, pre_rows, 128), cout=bf16(nz, rows * dt, 128),
+        cmid=bf16(nz, rows * dt, 128), cfin=bf16(nz, rows * dt, 128),
+        load_sem=sems(26), swap_s=sems(10), swap_r=sems(10), h_r=sems(3), g_r=sems(7), r_r=sems(nz - 1), one=sems(5), q_sem=sems(4), c_sem=sems(4),
     )
     outs = dict(o_out=like(A.hidden), o_state=like(A.state), o_window=like(A.window))
     vm, anywhere = pl.BlockSpec(memory_space=pltpu.VMEM), pl.BlockSpec(memory_space=pl.ANY)

time: 76.9 us -> 70.9 us (0.922)
  Pallas kernels: 75.9 us -> 70.1 us
    pallas_call x1, Pallas kernels: 73.1 us -> 67.3 us  [layer(): pl.pallas_call(functools.partial(kernel, nz, rows, inputs + tuple(outs) +...]
where the time goes in v2:
time: 70.9 us; the launch traced here: 70.7 us
  Pallas kernels  70.1 us (99%)
    pallas_call x1, Pallas kernels, layer(): pl.pallas_call(functools.partial(kernel, nz, rows, inputs + tuple(outs) +...  67.3 us
    pallas_call x1, Pallas kernels, layer(): pl.pallas_call(write_out, out_shape=tuple((jax.ShapeDtypeStruct(v.shape,...  2.76 us

profile of v2, /device:TPU:86, one launch (start us, length us, event | category | flops | bytes accessed | tf_op | source)
XLA Modules:
  0.0 70.7 jit_solution(5093486383798344767)
XLA Ops:
  0.6 67.3 %layer.1 = (bf16[3,2048]{1,0:T(4,128)(2,1)S(1)}, f32[96,128,128]{2,1,0:T(8,128)S(1)}, bf16[3,3,6144]{2,1,0:T(4,128)(2,1)S(1)}) custom-call(bf16[3,2048]{1,0:T(4,128)(2,1)} %refs_0_.1, bf16[3,3,6144]{2,1,0:T(4,128)(2,1)} %refs_1_.1, f32[96,128,128]{2,1,0:T(8,128)} %bitcast.14, bf16[2048,128]{1,0:T(8,128)(2,1)} %refs_3_.1, bf16[2048,128]{1,0:T(8,128)(2,1)} %refs_4_.1, ...), custom_call_target="tpu_custom_call" | custom-call | tf_op jit(solution)/shard_map/layer/pallas_call | solution.py:668
  68.0 2.8 %store.1 = (bf16[3,2048]{1,0:T(4,128)(2,1)}, f32[96,128,128]{2,1,0:T(8,128)}, bf16[3,3,6144]{2,1,0:T(4,128)(2,1)}) custom-call(bf16[3,2048]{1,0:T(4,128)(2,1)S(1)} %get-tuple-element.9.x, f32[96,128,128]{2,1,0:T(8,128)S(1)} %get-tuple-element.10.state, bf16[3,3,6144]{2,1,0:T(4,128)(2,1)S(1)} %get-tuple-element.11.window), custom_call_target="tpu_custom_call" | custom-call | tf_op jit(solution)/shard_map/store/pallas_call | solution.py:677

commit v3 on v2

--- a/solution.py
+++ b/solution.py
@@ -32,7 +32,7 @@
 
 
 def silu(v):
-    return v * (1.0 / (1.0 + jnp.exp(-v)))
+    return 0.5 * v * (1.0 + jnp.tanh(0.5 * v))
 
 
 def lanes(tiles):

time: 70.9 us -> 71 us (level)
  no operation moved by 1% of the time
where the time goes in v3:
time: 71 us; the launch traced here: 70.7 us
  Pallas kernels  70.1 us (99%)
    pallas_call x1, Pallas kernels, layer(): pl.pallas_call(functools.partial(kernel, nz, rows, inputs + tuple(outs) +...  67.3 us
    pallas_call x1, Pallas kernels, layer(): pl.pallas_call(write_out, out_shape=tuple((jax.ShapeDtypeStruct(v.shape,...  2.76 us

profile of v3, /device:TPU:86, one launch (start us, length us, event | category | flops | bytes accessed | tf_op | source)
XLA Modules:
  0.0 70.7 jit_solution(4864040595174162868)
XLA Ops:
  0.6 67.3 %layer.1 = (bf16[3,2048]{1,0:T(4,128)(2,1)S(1)}, f32[96,128,128]{2,1,0:T(8,128)S(1)}, bf16[3,3,6144]{2,1,0:T(4,128)(2,1)S(1)}) custom-call(bf16[3,2048]{1,0:T(4,128)(2,1)} %refs_0_.1, bf16[3,3,6144]{2,1,0:T(4,128)(2,1)} %refs_1_.1, f32[96,128,128]{2,1,0:T(8,128)} %bitcast.14, bf16[2048,128]{1,0:T(8,128)(2,1)} %refs_3_.1, bf16[2048,128]{1,0:T(8,128)(2,1)} %refs_4_.1, ...), custom_call_target="tpu_custom_call" | custom-call | tf_op jit(solution)/shard_map/layer/pallas_call | solution.py:668
  68.0 2.8 %store.1 = (bf16[3,2048]{1,0:T(4,128)(2,1)}, f32[96,128,128]{2,1,0:T(8,128)}, bf16[3,3,6144]{2,1,0:T(4,128)(2,1)}) custom-call(bf16[3,2048]{1,0:T(4,128)(2,1)S(1)} %get-tuple-element.9.x, f32[96,128,128]{2,1,0:T(8,128)S(1)} %get-tuple-element.10.state, bf16[3,3,6144]{2,1,0:T(4,128)(2,1)S(1)} %get-tuple-element.11.window), custom_call_target="tpu_custom_call" | custom-call | tf_op jit(solution)/shard_map/store/pallas_call | solution.py:677
